TPU v7x, 512 devices: a 8x2x16 block of a 8x16x16 slice. The times are simulated.
512 devices in a mesh: grp: 2 (over y), fs: 16 (over z), tp: 16 (over x, core).
Axes of the slice: x: 8, y: 2, z: 16, core: 2. Of those that a mesh axis runs over, the one named last changes fastest.
The devices are a block of a 8x16x16 slice.
Arguments:
- tokens: bfloat16 [16384, 2048], P(('grp', 'fs')), parts along dimension 0, may hold values from -6 to 6
- pre_gain: float32 [2048], replicated, may hold values from 0.1 to 1.9
- gate_weight: float32 [2048, 5632], P('fs', 'tp'), may hold values from -0.125 to 0.125
- gate_scale: float32 [5632], P('tp'), may hold values from 0.5 to 2
- up_weight: float32 [2048, 5632], P('fs', 'tp'), may hold values from -0.125 to 0.125
- up_scale: float32 [5632], P('tp'), may hold values from 0.5 to 2
- down_weight: float32 [5632, 2048], P('tp', 'fs'), may hold values from -0.078125 to 0.078125
- down_scale: float32 [2048], replicated, may hold values from 0.3 to 3
- post_gain: float32 [2048], replicated, may hold values from 0.1 to 1.9
Outputs:
- mixed: bfloat16 [16384, 2048], P(('grp', 'fs')), parts along dimension 0
There are 2 independent parts, one for each index of `grp`. A program takes and returns all parts, laid end to end along the dimension named above; an argument that names none is the same for every part. Nothing has to cross between parts.
All inputs are finite; a program needn't handle non-finite values.
Results may differ from a plain program's by a relative error of at most 0.018.
Values may be sent and summed in bfloat16 or wider, within the bound.
No kernel may reach another device: no remote copies, remote signals or barrier semaphores. Data moves between devices by JAX's collectives and lax.ppermute only.
A program may use at most 64 MiB of HBM per device.

v0:
```python
import jax
import jax.numpy as jnp
from jax import lax
from jax.experimental import pallas as pl
from jax.experimental.pallas import tpu as pltpu
from jax.sharding import PartitionSpec as P


EPS = 1e-06
LANES = 128
CORES = 2
ROWS = 256
CHUNKS = 1
FINISH_VMEM = 12 << 20
CHAINS = ("own", "other")


def flat(z, t, n_fs, n_tp):
    return (z % n_fs) * n_tp + t


def patterns(n_fs, n_tp):
    enter, own, ring = ([], [], [])
    for z in range(n_fs):
        for t in range(n_tp):
            here = flat(z, t, n_fs, n_tp)
            if t % CORES == 0:
                enter.append((here, flat(z - 1, t + 1, n_fs, n_tp)))
                ring.append((here, flat(z + 1, t, n_fs, n_tp)))
            else:
                enter.append((here, flat(z, t - 1, n_fs, n_tp)))
                own.append((here, flat(z - 1, t, n_fs, n_tp)))
                ring.append((here, flat(z - 1, t, n_fs, n_tp)))
    return enter, own, ring


def slab_of(slot, core, z, n_fs):
    return lax.rem(jnp.where(core == 0, z - slot + n_fs, z + 1 + slot), n_fs)


def finish_kernel(n_fs, place, mine, other, scale, gain, *outs):
    out = outs[-1]
    z, core = (place[0], place[1])
    slots = mine.shape[1] // LANES
    at_rows = pl.ds(pl.multiple_of(pl.program_id(0) * ROWS, ROWS), ROWS)
    total = None
    branches = []
    for held, which in ((mine, core), (other, 1 - core)):
        for k in range(slots):
            slab = slab_of(k, which, z, n_fs)
            branch = held[at_rows, k * LANES : (k + 1) * LANES].astype(jnp.float32)
            branch = branch * scale[pl.ds(slab, 1), :]
            squares = branch * branch
            total = squares if total is None else total + squares
            branches.append((slab, branch))
    width = LANES * len(branches)
    norm = lax.rsqrt(jnp.sum(total, axis=-1, keepdims=True) / width + EPS)
    for slab, branch in branches:
        at = pl.multiple_of(slab * LANES, LANES)
        out[:, pl.ds(at, LANES)] = (branch * norm * gain[pl.ds(slab, 1), :]).astype(out.dtype)


def finish(place, mine, other, scale, gain, n_fs, chunk, n_rows, done):
    rows, half = mine.shape
    first = chunk * rows // ROWS
    whole = pl.BlockSpec(memory_space=pltpu.VMEM)
    earlier = [] if done is None else [done]
    return pl.pallas_call(
        lambda *refs: finish_kernel(n_fs, *refs),
        grid_spec=pltpu.PrefetchScalarGridSpec(
            num_scalar_prefetch=1,
            grid=(rows // ROWS,),
            in_specs=[whole] * 4 + [pl.BlockSpec(memory_space=pl.ANY)] * len(earlier),
            out_specs=pl.BlockSpec((ROWS, 2 * half), lambda i, place: (first + i, 0)),
        ),
        out_shape=jax.ShapeDtypeStruct((n_rows, 2 * half), jnp.bfloat16),
        input_output_aliases={5: 0} if earlier else {},
        compiler_params=pltpu.CompilerParams(vmem_limit_bytes=FINISH_VMEM),
    )(place, mine, other, scale, gain, *earlier)


def body(
    tokens,
    pre_gain,
    gate_weight,
    gate_scale,
    up_weight,
    up_scale,
    down_weight,
    down_scale,
    post_gain,
):
    n_fs, n_tp = (lax.axis_size("fs"), lax.axis_size("tp"))
    both = ("fs", "tp")
    z, t = (lax.axis_index("fs"), lax.axis_index("tp"))
    core = t % CORES
    enter, own_first, ring = patterns(n_fs, n_tp)
    partner = [(i, i ^ 1) for i in range(n_tp)]
    chips = [[x * CORES + c for x in range(n_tp // CORES)] for c in range(CORES)]
    n_chips = n_tp // CORES
    low = jnp.bfloat16
    units = gate_weight.shape[1]

    packed = jnp.concatenate(
        [
            (gate_weight * gate_scale).astype(low).T,
            (up_weight * up_scale).astype(low).T,
            down_weight.astype(low),
        ],
        axis=0,
    )
    other0 = lax.ppermute(packed, both, enter)
    shifted = lax.ppermute(packed, both, own_first)
    own0 = jnp.where(core == 0, packed, shifted)

    rows = tokens.astype(jnp.float32)
    inverse = lax.rsqrt(jnp.mean(rows * rows, axis=-1, keepdims=True) + EPS)

    def normed_slab(k):
        slab = slab_of(k, core, z, n_fs)
        part = lax.dynamic_slice_in_dim(tokens, slab * LANES, LANES, axis=1).astype(jnp.float32)
        return (part * inverse * lax.dynamic_slice_in_dim(pre_gain, slab * LANES, LANES)).astype(low)

    def product(weights, k_normed):
        return lax.dot_general(
            weights, k_normed, (((1,), (1,)), ((), ())), preferred_element_type=jnp.float32
        )

    held = {"own": own0, "other": other0}

    def down_rows():
        return jnp.concatenate([held["own"][2 * units :], held["other"][2 * units :]], axis=0)

    downs = [down_rows()]
    slab = normed_slab(0)
    sum_own, sum_other = (product(held["own"][: 2 * units], slab), product(held["other"][: 2 * units], slab))
    for k in range(1, n_fs // 2):
        for chain in CHAINS:
            held[chain] = lax.ppermute(held[chain], both, ring)
        downs.append(down_rows())
        slab = normed_slab(k)
        sum_own = sum_own + product(held["own"][: 2 * units], slab)
        sum_other = sum_other + product(held["other"][: 2 * units], slab)

    sums = jnp.concatenate([sum_own, sum_other], axis=0).astype(low)
    arrived = lax.ppermute(sums, "tp", partner)

    def gated(sums, more):
        sums = sums + more.astype(jnp.float32)
        return (jax.nn.silu(sums[:units]) * sums[units:]).astype(low)

    hidden = jnp.concatenate(
        [gated(sum_own, arrived[2 * units :]), gated(sum_other, arrived[: 2 * units])], axis=0
    )
    columns = jnp.concatenate(downs, axis=1)

    n_rows = tokens.shape[0]
    lines = n_rows // CHUNKS
    scale, gain = (down_scale.reshape(-1, LANES), post_gain.reshape(-1, LANES))
    place = jnp.stack([z, core]).astype(jnp.int32)

    def over_chips(array):
        return lax.all_to_all(array, "tp", 0, 0, axis_index_groups=chips, tiled=True)

    parts = []
    for c in range(CHUNKS):
        partial = lax.dot_general(
            hidden[:, c * lines : (c + 1) * lines],
            columns,
            (((0,), (0,)), ((), ())),
            preferred_element_type=jnp.float32,
        ).astype(low)
        parts.append(over_chips(partial.reshape(n_chips, lines // n_chips, -1)))
    mines = []
    for part in parts:
        summed = jnp.sum(part.astype(jnp.float32), axis=0).astype(low)
        mines.append(over_chips(jnp.broadcast_to(summed, part.shape)).reshape(lines, -1))
    out = None
    for c, mine in enumerate(mines):
        other = lax.ppermute(mine, "tp", partner)
        out = finish(place, mine, other, scale, gain, n_fs, c, n_rows, out)
    return out


def solution(mesh):
    in_specs = (
        P(("grp", "fs"), None),
        P(),
        P("fs", "tp"),
        P("tp"),
        P("fs", "tp"),
        P("tp"),
        P("tp", "fs"),
        P(),
        P(),
    )
    out_specs = P(("grp", "fs"), None)

    return jax.shard_map(body, mesh=mesh, in_specs=in_specs, out_specs=out_specs, check_vma=False)
```

profile of v0, /device:TPU:65, one launch (start us, length us, event | category | flops | bytes accessed | tf_op | source)
XLA Modules:
  0.0 203.3 jit_solution(14204163894129124002)
XLA Ops:
  0.0 0.9 convert_element_type.80
  0.9 1.2 fusion.23
  2.2 41.5 %collective-permute-start.8 = (bf16[1056,128]{1,0:T(8,128)(2,1)S(1)}, bf16[1056,128]{1,0:T(8,128)(2,1)S(1)}, u32[]{:S(2)}, u32[]{:S(2)}) collective-permute-start(bf16[1056,128]{1,0:T(8,128)(2,1)S(1)} %pad_maximum_fusion.1), channel_id=1, source_target_pairs={{0,241},{1,0},{2,243},{3,2},{4,245},{5,4},{6,247},{7,6},{8,249},{9... | collective-permute-start | bytes 811016 | tf_op jit(solution)/shard_map/ppermute | solution.py:112
  43.7 3.7 %collective-permute-start = (bf16[1056,128]{1,0:T(8,128)(2,1)S(1)}, bf16[1056,128]{1,0:T(8,128)(2,1)S(1)}, u32[]{:S(2)}, u32[]{:S(2)}) collective-permute-start(bf16[1056,128]{1,0:T(8,128)(2,1)S(1)} %pad_maximum_fusion.1), channel_id=1, source_target_pairs={{1,241},{3,243},{5,245},{7,247},{9,249},{11,251},{13,253},{15,255}... | collective-permute-start | bytes 811016 | tf_op jit(solution)/shard_map/ppermute | solution.py:113
  47.4 2.1 %multiply_reduce_fusion = f32[512]{0:T(512)S(1)} fusion(bf16[512,2048]{1,0:T(8,128)(2,1)} %param.9), kind=kLoop, calls=%fused_computation | loop fusion | flops 3145216 | bytes 2099200 | tf_op jit(solution)/shard_map/reduce_sum | solution.py:117
  49.6 2.2 %collective-permute-done = bf16[1056,128]{1,0:T(8,128)(2,1)S(1)} collective-permute-done((bf16[1056,128]{1,0:T(8,128)(2,1)S(1)}, bf16[1056,128]{1,0:T(8,128)(2,1)S(1)}, u32[]{:S(2)}, u32[]{:S(2)}) %collective-permute-start) | collective-permute-done | bytes 270368 | tf_op jit(solution)/shard_map/ppermute | solution.py:113
  51.8 5.1 %collective-permute-start.1 = (bf16[1056,128]{1,0:T(8,128)(2,1)S(1)}, bf16[1056,128]{1,0:T(8,128)(2,1)S(1)}, u32[]{:S(2)}, u32[]{:S(2)}) collective-permute-start(bf16[1056,128]{1,0:T(8,128)(2,1)S(1)} %broadcast_select_fusion), channel_id=1, source_target_pairs={{0,16},{1,241},{2,18},{3,243},{4,20},{5,245},{6,22},{7,247},{8,24}... | collective-permute-start | bytes 811016 | tf_op jit(solution)/shard_map/ppermute | solution.py:139
  57.0 1.9 collective-permute-start.9
  59.4 0.8 collective-permute-done.1
  60.3 5.0 %collective-permute-start.2 = (bf16[1056,128]{1,0:T(8,128)(2,1)S(1)}, bf16[1056,128]{1,0:T(8,128)(2,1)S(1)}, u32[]{:S(2)}, u32[]{:S(2)}) collective-permute-start(bf16[1056,128]{1,0:T(8,128)(2,1)S(1)} %collective-permute-done.1), channel_id=1, source_target_pairs={{0,16},{1,241},{2,18},{3,243},{4,20},{5,245},{6,22},{7,247},{8,24}... | collective-permute-start | bytes 811016 | tf_op jit(solution)/shard_map/ppermute | solution.py:139
  65.3 0.5 fusion.20
  65.8 0.5 convolution_add_fusion.13
  66.2 2.0 collective-permute-start.10
  68.2 0.5 convolution_add_fusion.6
  68.7 4.8 %collective-permute-done.10 = bf16[1056,128]{1,0:T(8,128)(2,1)S(1)} collective-permute-done((bf16[1056,128]{1,0:T(8,128)(2,1)S(1)}, bf16[1056,128]{1,0:T(8,128)(2,1)S(1)}, u32[]{:S(2)}, u32[]{:S(2)}) %collective-permute-start.10) | collective-permute-done | bytes 270368 | tf_op jit(solution)/shard_map/ppermute | solution.py:139
  73.5 3.1 %collective-permute-start.11 = (bf16[1056,128]{1,0:T(8,128)(2,1)S(1)}, bf16[1056,128]{1,0:T(8,128)(2,1)S(1)}, u32[]{:S(2)}, u32[]{:S(2)}) collective-permute-start(bf16[1056,128]{1,0:T(8,128)(2,1)S(1)} %collective-permute-done.10), channel_id=1, source_target_pairs={{0,16},{1,241},{2,18},{3,243},{4,20},{5,245},{6,22},{7,247},{8,24}... | collective-permute-start | bytes 811016 | tf_op jit(solution)/shard_map/ppermute | solution.py:139
  76.6 2.0 collective-permute-start.3
  78.6 0.5 convolution_add_fusion.12
  79.1 0.5 convolution_add_fusion.5
  79.5 1.5 collective-permute-done.11
  81.0 4.1 %collective-permute-start.12 = (bf16[1056,128]{1,0:T(8,128)(2,1)S(1)}, bf16[1056,128]{1,0:T(8,128)(2,1)S(1)}, u32[]{:S(2)}, u32[]{:S(2)}) collective-permute-start(bf16[1056,128]{1,0:T(8,128)(2,1)S(1)} %collective-permute-done.11), channel_id=1, source_target_pairs={{0,16},{1,241},{2,18},{3,243},{4,20},{5,245},{6,22},{7,247},{8,24}... | collective-permute-start | bytes 811016 | tf_op jit(solution)/shard_map/ppermute | solution.py:139
  85.1 2.9 %collective-permute-start.4 = (bf16[1056,128]{1,0:T(8,128)(2,1)S(1)}, bf16[1056,128]{1,0:T(8,128)(2,1)S(1)}, u32[]{:S(2)}, u32[]{:S(2)}) collective-permute-start(bf16[1056,128]{1,0:T(8,128)(2,1)S(1)} %collective-permute-done.3), channel_id=1, source_target_pairs={{0,16},{1,241},{2,18},{3,243},{4,20},{5,245},{6,22},{7,247},{8,24}... | collective-permute-start | bytes 811016 | tf_op jit(solution)/shard_map/ppermute | solution.py:139
  88.0 0.5 convolution_add_fusion.11
  88.4 0.5 convolution_add_fusion.4
  88.9 4.6 %collective-permute-start.13 = (bf16[1056,128]{1,0:T(8,128)(2,1)S(1)}, bf16[1056,128]{1,0:T(8,128)(2,1)S(1)}, u32[]{:S(2)}, u32[]{:S(2)}) collective-permute-start(bf16[1056,128]{1,0:T(8,128)(2,1)S(1)} %collective-permute-done.12), channel_id=1, source_target_pairs={{0,16},{1,241},{2,18},{3,243},{4,20},{5,245},{6,22},{7,247},{8,24}... | collective-permute-start | bytes 811016 | tf_op jit(solution)/shard_map/ppermute | solution.py:139
  93.5 2.9 %collective-permute-start.5 = (bf16[1056,128]{1,0:T(8,128)(2,1)S(1)}, bf16[1056,128]{1,0:T(8,128)(2,1)S(1)}, u32[]{:S(2)}, u32[]{:S(2)}) collective-permute-start(bf16[1056,128]{1,0:T(8,128)(2,1)S(1)} %collective-permute-done.4), channel_id=1, source_target_pairs={{0,16},{1,241},{2,18},{3,243},{4,20},{5,245},{6,22},{7,247},{8,24}... | collective-permute-start | bytes 811016 | tf_op jit(solution)/shard_map/ppermute | solution.py:139
  96.4 0.5 convolution_add_fusion.10
  96.9 0.5 convolution_add_fusion.3
  97.3 4.6 %collective-permute-start.14 = (bf16[1056,128]{1,0:T(8,128)(2,1)S(1)}, bf16[1056,128]{1,0:T(8,128)(2,1)S(1)}, u32[]{:S(2)}, u32[]{:S(2)}) collective-permute-start(bf16[1056,128]{1,0:T(8,128)(2,1)S(1)} %collective-permute-done.13), channel_id=1, source_target_pairs={{0,16},{1,241},{2,18},{3,243},{4,20},{5,245},{6,22},{7,247},{8,24}... | collective-permute-start | bytes 811016 | tf_op jit(solution)/shard_map/ppermute | solution.py:139
  102.0 2.9 %collective-permute-start.6 = (bf16[1056,128]{1,0:T(8,128)(2,1)S(1)}, bf16[1056,128]{1,0:T(8,128)(2,1)S(1)}, u32[]{:S(2)}, u32[]{:S(2)}) collective-permute-start(bf16[1056,128]{1,0:T(8,128)(2,1)S(1)} %collective-permute-done.5), channel_id=1, source_target_pairs={{0,16},{1,241},{2,18},{3,243},{4,20},{5,245},{6,22},{7,247},{8,24}... | collective-permute-start | bytes 811016 | tf_op jit(solution)/shard_map/ppermute | solution.py:139
  104.8 0.5 convolution_add_fusion.9
  105.3 0.5 convolution_add_fusion.2
  105.8 4.6 %collective-permute-start.15 = (bf16[1056,128]{1,0:T(8,128)(2,1)S(1)}, bf16[1056,128]{1,0:T(8,128)(2,1)S(1)}, u32[]{:S(2)}, u32[]{:S(2)}) collective-permute-start(bf16[1056,128]{1,0:T(8,128)(2,1)S(1)} %collective-permute-done.14), channel_id=1, source_target_pairs={{0,16},{1,241},{2,18},{3,243},{4,20},{5,245},{6,22},{7,247},{8,24}... | collective-permute-start | bytes 811016 | tf_op jit(solution)/shard_map/ppermute | solution.py:139
  110.4 2.9 %collective-permute-start.7 = (bf16[1056,128]{1,0:T(8,128)(2,1)S(1)}, bf16[1056,128]{1,0:T(8,128)(2,1)S(1)}, u32[]{:S(2)}, u32[]{:S(2)}) collective-permute-start(bf16[1056,128]{1,0:T(8,128)(2,1)S(1)} %collective-permute-done.6), channel_id=1, source_target_pairs={{0,16},{1,241},{2,18},{3,243},{4,20},{5,245},{6,22},{7,247},{8,24}... | collective-permute-start | bytes 811016 | tf_op jit(solution)/shard_map/ppermute | solution.py:139
  113.3 0.5 convolution_add_fusion.8
  113.7 0.5 convolution_add_fusion.1
  114.2 3.7 %collective-permute-done.7 = bf16[1056,128]{1,0:T(8,128)(2,1)S(1)} collective-permute-done((bf16[1056,128]{1,0:T(8,128)(2,1)S(1)}, bf16[1056,128]{1,0:T(8,128)(2,1)S(1)}, u32[]{:S(2)}, u32[]{:S(2)}) %collective-permute-start.7) | collective-permute-done | bytes 270368 | tf_op jit(solution)/shard_map/ppermute | solution.py:139
  117.9 0.5 fusion.44
  118.4 0.5 fusion.43
  119.0 5.1 %collective-permute-start.16 = (bf16[1408,512]{1,0:T(8,128)(2,1)S(1)}, bf16[1408,512]{1,0:T(8,128)(2,1)S(1)}, u32[]{:S(2)}, u32[]{:S(2)}) collective-permute-start(bf16[1408,512]{1,0:T(8,128)(2,1)S(1)} %pad_maximum_fusion), channel_id=1, source_target_pairs={{0,1},{1,0},{2,3},{3,2},{4,5},{5,4},{6,7},{7,6},{8,9},{9,8},{10,11... | collective-permute-start | bytes 4325384 | tf_op jit(solution)/shard_map/ppermute | solution.py:146
  124.8 2.1 %collective-permute-done.16 = bf16[1408,512]{1,0:T(8,128)(2,1)S(1)} collective-permute-done((bf16[1408,512]{1,0:T(8,128)(2,1)S(1)}, bf16[1408,512]{1,0:T(8,128)(2,1)S(1)}, u32[]{:S(2)}, u32[]{:S(2)}) %collective-permute-start.16) | collective-permute-done | bytes 1441824 | tf_op jit(solution)/shard_map/ppermute | solution.py:146
  126.9 0.5 convert_add_fusion.1
  127.9 1.0 convolution_convert_fusion
  128.9 34.8 %all_to_all.10 = bf16[8,64,1024]{2,1,0:T(8,128)(2,1)S(1)} all-to-all(bf16[8,64,1024]{2,1,0:T(8,128)(2,1)S(1)} %bitcast.15), channel_id=1, replica_groups={{0,2,4,6,8,10,12,14},{1,3,5,7,9,11,13,15},{16,18,20,22,24,26,28,30},{17..., dimensions={0} | all-to-all | bytes 2097152 | tf_op jit(solution)/shard_map/all_to_all | solution.py:163
  164.0 28.8 %all_to_all.11 = bf16[8,64,1024]{2,1,0:T(8,128)(2,1)S(1)} all-to-all(bf16[8,64,1024]{2,1,0:T(8,128)(2,1)S(1)} %broadcast_in_dim.2), channel_id=1, replica_groups={{0,2,4,6,8,10,12,14},{1,3,5,7,9,11,13,15},{16,18,20,22,24,26,28,30},{17..., dimensions={0} | all-to-all | bytes 2097152 | tf_op jit(solution)/shard_map/all_to_all | solution.py:163
  192.8 5.2 %collective-permute-start.17 = (bf16[512,1024]{1,0:T(8,128)(2,1)S(1)}, bf16[512,1024]{1,0:T(8,128)(2,1)S(1)}, u32[]{:S(2)}, u32[]{:S(2)}) collective-permute-start(bf16[512,1024]{1,0:T(8,128)(2,1)S(1)} %bitcast.11), channel_id=1, source_target_pairs={{0,1},{1,0},{2,3},{3,2},{4,5},{5,4},{6,7},{7,6},{8,9},{9,8},{10,11... | collective-permute-start | bytes 3145736 | tf_op jit(solution)/shard_map/ppermute | solution.py:180
  198.1 2.2 %collective-permute-done.17.refs_2_ = bf16[512,1024]{1,0:T(8,128)(2,1)S(1)} collective-permute-done((bf16[512,1024]{1,0:T(8,128)(2,1)S(1)}, bf16[512,1024]{1,0:T(8,128)(2,1)S(1)}, u32[]{:S(2)}, u32[]{:S(2)}) %collective-permute-start.17) | collective-permute-done | bytes 1048608 | tf_op jit(solution)/shard_map/ppermute | solution.py:180
  200.3 2.9 %shard_map.91 = bf16[512,2048]{1,0:T(8,128)(2,1)} custom-call(s32[2]{0:T(128)S(1)} %pad_add_fusion.refs_0_, bf16[512,1024]{1,0:T(8,128)(2,1)S(1)} %bitcast.12, bf16[512,1024]{1,0:T(8,128)(2,1)S(1)} %collective-permute-done.17.refs_2_, f32[16,128]{1,0:T(8,128)S(1)} %bitcast.13, f32[16,128]{1,0:T(8,128)S(1)} %bitcast.14), custom_call_target="tpu_custom_call" | custom-call | tf_op jit(solution)/shard_map/pallas_call | solution.py:68
  (54 shorter events, 2.2 us)
Async XLA Ops:
  2.2 54.7 %copy-start.3 = (f32[2048]{0:T(1024)S(1)}, f32[2048]{0:T(1024)}, u32[]{:S(2)}) copy-start(f32[2048]{0:T(1024)} %param.10) | copy-start | bytes 24580
  2.2 56.8 %copy-start.2 = (bf16[512,2048]{1,0:T(8,128)(2,1)S(1)}, bf16[512,2048]{1,0:T(8,128)(2,1)}, u32[]{:S(2)}) copy-start(bf16[512,2048]{1,0:T(8,128)(2,1)} %param.9) | copy-start | bytes 6291460
  2.2 54.8 %collective-permute-start.8 = (bf16[1056,128]{1,0:T(8,128)(2,1)S(1)}, bf16[1056,128]{1,0:T(8,128)(2,1)S(1)}, u32[]{:S(2)}, u32[]{:S(2)}) collective-permute-start(bf16[1056,128]{1,0:T(8,128)(2,1)S(1)} %pad_maximum_fusion.1), channel_id=1, source_target_pairs={{0,241},{1,0},{2,243},{3,2},{4,245},{5,4},{6,247},{7,6},{8,249},{9... | collective-permute-start | bytes 811016 | tf_op jit(solution)/shard_map/ppermute | solution.py:112
  43.7 8.1 %collective-permute-start = (bf16[1056,128]{1,0:T(8,128)(2,1)S(1)}, bf16[1056,128]{1,0:T(8,128)(2,1)S(1)}, u32[]{:S(2)}, u32[]{:S(2)}) collective-permute-start(bf16[1056,128]{1,0:T(8,128)(2,1)S(1)} %pad_maximum_fusion.1), channel_id=1, source_target_pairs={{1,241},{3,243},{5,245},{7,247},{9,249},{11,251},{13,253},{15,255}... | collective-permute-start | bytes 811016 | tf_op jit(solution)/shard_map/ppermute | solution.py:113
  51.8 8.4 %collective-permute-start.1 = (bf16[1056,128]{1,0:T(8,128)(2,1)S(1)}, bf16[1056,128]{1,0:T(8,128)(2,1)S(1)}, u32[]{:S(2)}, u32[]{:S(2)}) collective-permute-start(bf16[1056,128]{1,0:T(8,128)(2,1)S(1)} %broadcast_select_fusion), channel_id=1, source_target_pairs={{0,16},{1,241},{2,18},{3,243},{4,20},{5,245},{6,22},{7,247},{8,24}... | collective-permute-start | bytes 811016 | tf_op jit(solution)/shard_map/ppermute | solution.py:139
  57.0 9.2 %collective-permute-start.9 = (bf16[1056,128]{1,0:T(8,128)(2,1)S(1)}, bf16[1056,128]{1,0:T(8,128)(2,1)S(1)}, u32[]{:S(2)}, u32[]{:S(2)}) collective-permute-start(bf16[1056,128]{1,0:T(8,128)(2,1)S(1)} %collective-permute-done.8), channel_id=1, source_target_pairs={{0,16},{1,241},{2,18},{3,243},{4,20},{5,245},{6,22},{7,247},{8,24}... | collective-permute-start | bytes 811016 | tf_op jit(solution)/shard_map/ppermute | solution.py:139
  60.3 16.4 %collective-permute-start.2 = (bf16[1056,128]{1,0:T(8,128)(2,1)S(1)}, bf16[1056,128]{1,0:T(8,128)(2,1)S(1)}, u32[]{:S(2)}, u32[]{:S(2)}) collective-permute-start(bf16[1056,128]{1,0:T(8,128)(2,1)S(1)} %collective-permute-done.1), channel_id=1, source_target_pairs={{0,16},{1,241},{2,18},{3,243},{4,20},{5,245},{6,22},{7,247},{8,24}... | collective-permute-start | bytes 811016 | tf_op jit(solution)/shard_map/ppermute | solution.py:139
  66.2 7.2 %collective-permute-start.10 = (bf16[1056,128]{1,0:T(8,128)(2,1)S(1)}, bf16[1056,128]{1,0:T(8,128)(2,1)S(1)}, u32[]{:S(2)}, u32[]{:S(2)}) collective-permute-start(bf16[1056,128]{1,0:T(8,128)(2,1)S(1)} %collective-permute-done.9), channel_id=1, source_target_pairs={{0,16},{1,241},{2,18},{3,243},{4,20},{5,245},{6,22},{7,247},{8,24}... | collective-permute-start | bytes 811016 | tf_op jit(solution)/shard_map/ppermute | solution.py:139
  73.5 7.5 %collective-permute-start.11 = (bf16[1056,128]{1,0:T(8,128)(2,1)S(1)}, bf16[1056,128]{1,0:T(8,128)(2,1)S(1)}, u32[]{:S(2)}, u32[]{:S(2)}) collective-permute-start(bf16[1056,128]{1,0:T(8,128)(2,1)S(1)} %collective-permute-done.10), channel_id=1, source_target_pairs={{0,16},{1,241},{2,18},{3,243},{4,20},{5,245},{6,22},{7,247},{8,24}... | collective-permute-start | bytes 811016 | tf_op jit(solution)/shard_map/ppermute | solution.py:139
  76.6 8.4 %collective-permute-start.3 = (bf16[1056,128]{1,0:T(8,128)(2,1)S(1)}, bf16[1056,128]{1,0:T(8,128)(2,1)S(1)}, u32[]{:S(2)}, u32[]{:S(2)}) collective-permute-start(bf16[1056,128]{1,0:T(8,128)(2,1)S(1)} %collective-permute-done.2), channel_id=1, source_target_pairs={{0,16},{1,241},{2,18},{3,243},{4,20},{5,245},{6,22},{7,247},{8,24}... | collective-permute-start | bytes 811016 | tf_op jit(solution)/shard_map/ppermute | solution.py:139
  81.0 7.9 %collective-permute-start.12 = (bf16[1056,128]{1,0:T(8,128)(2,1)S(1)}, bf16[1056,128]{1,0:T(8,128)(2,1)S(1)}, u32[]{:S(2)}, u32[]{:S(2)}) collective-permute-start(bf16[1056,128]{1,0:T(8,128)(2,1)S(1)} %collective-permute-done.11), channel_id=1, source_target_pairs={{0,16},{1,241},{2,18},{3,243},{4,20},{5,245},{6,22},{7,247},{8,24}... | collective-permute-start | bytes 811016 | tf_op jit(solution)/shard_map/ppermute | solution.py:139
  85.1 8.4 %collective-permute-start.4 = (bf16[1056,128]{1,0:T(8,128)(2,1)S(1)}, bf16[1056,128]{1,0:T(8,128)(2,1)S(1)}, u32[]{:S(2)}, u32[]{:S(2)}) collective-permute-start(bf16[1056,128]{1,0:T(8,128)(2,1)S(1)} %collective-permute-done.3), channel_id=1, source_target_pairs={{0,16},{1,241},{2,18},{3,243},{4,20},{5,245},{6,22},{7,247},{8,24}... | collective-permute-start | bytes 811016 | tf_op jit(solution)/shard_map/ppermute | solution.py:139
  88.9 8.4 %collective-permute-start.13 = (bf16[1056,128]{1,0:T(8,128)(2,1)S(1)}, bf16[1056,128]{1,0:T(8,128)(2,1)S(1)}, u32[]{:S(2)}, u32[]{:S(2)}) collective-permute-start(bf16[1056,128]{1,0:T(8,128)(2,1)S(1)} %collective-permute-done.12), channel_id=1, source_target_pairs={{0,16},{1,241},{2,18},{3,243},{4,20},{5,245},{6,22},{7,247},{8,24}... | collective-permute-start | bytes 811016 | tf_op jit(solution)/shard_map/ppermute | solution.py:139
  93.5 8.4 %collective-permute-start.5 = (bf16[1056,128]{1,0:T(8,128)(2,1)S(1)}, bf16[1056,128]{1,0:T(8,128)(2,1)S(1)}, u32[]{:S(2)}, u32[]{:S(2)}) collective-permute-start(bf16[1056,128]{1,0:T(8,128)(2,1)S(1)} %collective-permute-done.4), channel_id=1, source_target_pairs={{0,16},{1,241},{2,18},{3,243},{4,20},{5,245},{6,22},{7,247},{8,24}... | collective-permute-start | bytes 811016 | tf_op jit(solution)/shard_map/ppermute | solution.py:139
  97.3 8.4 %collective-permute-start.14 = (bf16[1056,128]{1,0:T(8,128)(2,1)S(1)}, bf16[1056,128]{1,0:T(8,128)(2,1)S(1)}, u32[]{:S(2)}, u32[]{:S(2)}) collective-permute-start(bf16[1056,128]{1,0:T(8,128)(2,1)S(1)} %collective-permute-done.13), channel_id=1, source_target_pairs={{0,16},{1,241},{2,18},{3,243},{4,20},{5,245},{6,22},{7,247},{8,24}... | collective-permute-start | bytes 811016 | tf_op jit(solution)/shard_map/ppermute | solution.py:139
  102.0 8.4 %collective-permute-start.6 = (bf16[1056,128]{1,0:T(8,128)(2,1)S(1)}, bf16[1056,128]{1,0:T(8,128)(2,1)S(1)}, u32[]{:S(2)}, u32[]{:S(2)}) collective-permute-start(bf16[1056,128]{1,0:T(8,128)(2,1)S(1)} %collective-permute-done.5), channel_id=1, source_target_pairs={{0,16},{1,241},{2,18},{3,243},{4,20},{5,245},{6,22},{7,247},{8,24}... | collective-permute-start | bytes 811016 | tf_op jit(solution)/shard_map/ppermute | solution.py:139
  105.8 12.6 %collective-permute-start.15 = (bf16[1056,128]{1,0:T(8,128)(2,1)S(1)}, bf16[1056,128]{1,0:T(8,128)(2,1)S(1)}, u32[]{:S(2)}, u32[]{:S(2)}) collective-permute-start(bf16[1056,128]{1,0:T(8,128)(2,1)S(1)} %collective-permute-done.14), channel_id=1, source_target_pairs={{0,16},{1,241},{2,18},{3,243},{4,20},{5,245},{6,22},{7,247},{8,24}... | collective-permute-start | bytes 811016 | tf_op jit(solution)/shard_map/ppermute | solution.py:139
  110.4 7.5 %collective-permute-start.7 = (bf16[1056,128]{1,0:T(8,128)(2,1)S(1)}, bf16[1056,128]{1,0:T(8,128)(2,1)S(1)}, u32[]{:S(2)}, u32[]{:S(2)}) collective-permute-start(bf16[1056,128]{1,0:T(8,128)(2,1)S(1)} %collective-permute-done.6), channel_id=1, source_target_pairs={{0,16},{1,241},{2,18},{3,243},{4,20},{5,245},{6,22},{7,247},{8,24}... | collective-permute-start | bytes 811016 | tf_op jit(solution)/shard_map/ppermute | solution.py:139
  119.0 7.9 %collective-permute-start.16 = (bf16[1408,512]{1,0:T(8,128)(2,1)S(1)}, bf16[1408,512]{1,0:T(8,128)(2,1)S(1)}, u32[]{:S(2)}, u32[]{:S(2)}) collective-permute-start(bf16[1408,512]{1,0:T(8,128)(2,1)S(1)} %pad_maximum_fusion), channel_id=1, source_target_pairs={{0,1},{1,0},{2,3},{3,2},{4,5},{5,4},{6,7},{7,6},{8,9},{9,8},{10,11... | collective-permute-start | bytes 4325384 | tf_op jit(solution)/shard_map/ppermute | solution.py:146
  163.8 36.5 %copy-start = (f32[2048]{0:T(1024)S(1)}, f32[2048]{0:T(1024)}, u32[]{:S(2)}) copy-start(f32[2048]{0:T(1024)} %param.16) | copy-start | bytes 24580
  163.9 36.5 %copy-start.1 = (f32[2048]{0:T(1024)S(1)}, f32[2048]{0:T(1024)}, u32[]{:S(2)}) copy-start(f32[2048]{0:T(1024)} %param.17) | copy-start | bytes 24580
  192.8 7.5 %collective-permute-start.17 = (bf16[512,1024]{1,0:T(8,128)(2,1)S(1)}, bf16[512,1024]{1,0:T(8,128)(2,1)S(1)}, u32[]{:S(2)}, u32[]{:S(2)}) collective-permute-start(bf16[512,1024]{1,0:T(8,128)(2,1)S(1)} %bitcast.11), channel_id=1, source_target_pairs={{0,1},{1,0},{2,3},{3,2},{4,5},{5,4},{6,7},{7,6},{8,9},{9,8},{10,11... | collective-permute-start | bytes 3145736 | tf_op jit(solution)/shard_map/ppermute | solution.py:180
where the time goes:
time: 204 us; the launch traced here: 203 us
  starting transfers between devices  104 us (51%)
  blocking collectives  63.6 us (31%)
  waiting for transfers between devices  17.3 us (8%)
  matrix products  8.32 us (4%)
  other arithmetic  6.01 us (3%)
  Pallas kernels  2.95 us (1%)
    all_to_all x2, blocking collectives, over_chips(): lax.all_to_all(array, 'tp', 0, 0, axis_index_groups=chips, tiled=True)  63.6 us
    ppermute x14, starting transfers between devices, body(): held[chain] = lax.ppermute(held[chain], both, ring)  48.4 us
    ppermute x1, starting transfers between devices, body(): other0 = lax.ppermute(packed, both, enter)  41.5 us
    ppermute x14, waiting for transfers between devices, body(): held[chain] = lax.ppermute(held[chain], both, ring)  10.8 us
    dot_general x16, matrix products, product(): lax.dot_general(weights, k_normed, (((1,), (1,)), ((), ())), preferred_el...  7.32 us
    ppermute x1, starting transfers between devices, body(): other = lax.ppermute(mine, 'tp', partner)  5.25 us
    ppermute x1, starting transfers between devices, body(): arrived = lax.ppermute(sums, 'tp', partner)  5.11 us
  transfers between devices with their start and end apart: 18, of which 7 were waited for; matrix products, arithmetic and copies ran while one was open for 5% of the time, Pallas kernels for 0%

commit v1 on v0

--- a/solution.py
+++ b/solution.py
@@ -12,7 +12,7 @@
 ROWS = 256
 CHUNKS = 1
 FINISH_VMEM = 12 << 20
-CHAINS = ("own", "other")
+WHOLE = 3
 
 
 def flat(z, t, n_fs, n_tp):
@@ -32,6 +32,10 @@
                 own.append((here, flat(z - 1, t, n_fs, n_tp)))
                 ring.append((here, flat(z - 1, t, n_fs, n_tp)))
     return enter, own, ring
+
+
+def chains_of(k):
+    return ("own", "other") if k <= WHOLE else ("own", "other", "down")
 
 
 def slab_of(slot, core, z, n_fs):
@@ -135,9 +139,11 @@
     slab = normed_slab(0)
     sum_own, sum_other = (product(held["own"][: 2 * units], slab), product(held["other"][: 2 * units], slab))
     for k in range(1, n_fs // 2):
-        for chain in CHAINS:
+        if k == WHOLE + 1:
+            held = {"own": held["own"][: 2 * units], "other": held["other"][: 2 * units], "down": downs[-1]}
+        for chain in chains_of(k):
             held[chain] = lax.ppermute(held[chain], both, ring)
-        downs.append(down_rows())
+        downs.append(down_rows() if k <= WHOLE else held["down"])
         slab = normed_slab(k)
         sum_own = sum_own + product(held["own"][: 2 * units], slab)
         sum_other = sum_other + product(held["other"][: 2 * units], slab)
@@ -146,8 +152,9 @@
     arrived = lax.ppermute(sums, "tp", partner)
 
     def gated(sums, more):
-        sums = sums + more.astype(jnp.float32)
-        return (jax.nn.silu(sums[:units]) * sums[units:]).astype(low)
+        gate = sums[:units] + more[:units].astype(jnp.float32)
+        up = sums[units:] + more[units:].astype(jnp.float32)
+        return (jax.nn.silu(gate) * up).astype(low)
 
     hidden = jnp.concatenate(
         [gated(sum_own, arrived[2 * units :]), gated(sum_other, arrived[: 2 * units])], axis=0

time: 204 us -> 222 us (1.088)
  starting transfers between devices: 104 us -> 123 us
  blocking collectives: 63.6 us -> 51.5 us
  waiting for transfers between devices: 17.3 us -> 28.1 us
    ppermute x14 -> x18, waiting for transfers between devices: 10.8 us -> 23.7 us  [body(): held[chain] = lax.ppermute(held[chain], both, ring)]
    ppermute x14 -> x18, starting transfers between devices: 48.4 us -> 61.3 us  [body(): held[chain] = lax.ppermute(held[chain], both, ring)]
    all_to_all x2, blocking collectives: 63.6 us -> 51.5 us  [over_chips(): lax.all_to_all(array, 'tp', 0, 0, axis_index_groups=chips, tiled=True)]
    ppermute x1, starting transfers between devices: 5.25 us -> 11.4 us  [body(): other = lax.ppermute(mine, 'tp', partner)]
  transfers between devices with their start and end apart: 18 -> 22, of which waited for: 7 -> 10; matrix products, arithmetic and copies ran while one was open for 5% -> 4% of each run, Pallas kernels for 0% -> 0%
where the time goes in v1:
time: 222 us; the launch traced here: 221 us
  starting transfers between devices  123 us (55%)
  blocking collectives  51.5 us (23%)
  waiting for transfers between devices  28.1 us (13%)
  matrix products  8.33 us (4%)
  other arithmetic  5.42 us (2%)
  Pallas kernels  2.95 us (1%)
    ppermute x18, starting transfers between devices, body(): held[chain] = lax.ppermute(held[chain], both, ring)  61.3 us
    all_to_all x2, blocking collectives, over_chips(): lax.all_to_all(array, 'tp', 0, 0, axis_index_groups=chips, tiled=True)  51.5 us
    ppermute x1, starting transfers between devices, body(): other0 = lax.ppermute(packed, both, enter)  41.5 us
    ppermute x18, waiting for transfers between devices, body(): held[chain] = lax.ppermute(held[chain], both, ring)  23.7 us
    ppermute x1, starting transfers between devices, body(): other = lax.ppermute(mine, 'tp', partner)  11.4 us
    dot_general x16, matrix products, product(): lax.dot_general(weights, k_normed, (((1,), (1,)), ((), ())), preferred_el...  7.33 us
    ppermute x1, starting transfers between devices, body(): arrived = lax.ppermute(sums, 'tp', partner)  5.27 us
  transfers between devices with their start and end apart: 22, of which 10 were waited for; matrix products, arithmetic and copies ran while one was open for 4% of the time, Pallas kernels for 0%

profile of v1, /device:TPU:65, one launch (start us, length us, event | category | flops | bytes accessed | tf_op | source)
XLA Modules:
  0.0 220.7 jit_solution(12430172521679355888)
XLA Ops:
  0.0 0.9 convert_element_type.86
  0.9 1.2 fusion.17
  2.2 41.5 %collective-permute-start.8 = (bf16[1056,128]{1,0:T(8,128)(2,1)S(1)}, bf16[1056,128]{1,0:T(8,128)(2,1)S(1)}, u32[]{:S(2)}, u32[]{:S(2)}) collective-permute-start(bf16[1056,128]{1,0:T(8,128)(2,1)S(1)} %pad_maximum_fusion.1), channel_id=1, source_target_pairs={{0,241},{1,0},{2,243},{3,2},{4,245},{5,4},{6,247},{7,6},{8,249},{9... | collective-permute-start | bytes 811016 | tf_op jit(solution)/shard_map/ppermute | solution.py:116
  43.7 3.7 %collective-permute-start = (bf16[1056,128]{1,0:T(8,128)(2,1)S(1)}, bf16[1056,128]{1,0:T(8,128)(2,1)S(1)}, u32[]{:S(2)}, u32[]{:S(2)}) collective-permute-start(bf16[1056,128]{1,0:T(8,128)(2,1)S(1)} %pad_maximum_fusion.1), channel_id=1, source_target_pairs={{1,241},{3,243},{5,245},{7,247},{9,249},{11,251},{13,253},{15,255}... | collective-permute-start | bytes 811016 | tf_op jit(solution)/shard_map/ppermute | solution.py:117
  47.4 2.1 multiply_reduce_fusion
  49.6 2.2 collective-permute-done
  51.8 5.1 %collective-permute-start.1 = (bf16[1056,128]{1,0:T(8,128)(2,1)S(1)}, bf16[1056,128]{1,0:T(8,128)(2,1)S(1)}, u32[]{:S(2)}, u32[]{:S(2)}) collective-permute-start(bf16[1056,128]{1,0:T(8,128)(2,1)S(1)} %broadcast_select_fusion), channel_id=1, source_target_pairs={{0,16},{1,241},{2,18},{3,243},{4,20},{5,245},{6,22},{7,247},{8,24}... | collective-permute-start | bytes 811016 | tf_op jit(solution)/shard_map/ppermute | solution.py:145
  57.0 1.9 collective-permute-start.9
  59.4 0.8 collective-permute-done.1
  60.3 5.0 %collective-permute-start.2 = (bf16[1056,128]{1,0:T(8,128)(2,1)S(1)}, bf16[1056,128]{1,0:T(8,128)(2,1)S(1)}, u32[]{:S(2)}, u32[]{:S(2)}) collective-permute-start(bf16[1056,128]{1,0:T(8,128)(2,1)S(1)} %collective-permute-done.1), channel_id=1, source_target_pairs={{0,16},{1,241},{2,18},{3,243},{4,20},{5,245},{6,22},{7,247},{8,24}... | collective-permute-start | bytes 811016 | tf_op jit(solution)/shard_map/ppermute | solution.py:145
  66.2 2.0 collective-permute-start.10
  68.7 4.8 %collective-permute-done.10 = bf16[1056,128]{1,0:T(8,128)(2,1)S(1)} collective-permute-done((bf16[1056,128]{1,0:T(8,128)(2,1)S(1)}, bf16[1056,128]{1,0:T(8,128)(2,1)S(1)}, u32[]{:S(2)}, u32[]{:S(2)}) %collective-permute-start.10) | collective-permute-done | bytes 270368 | tf_op jit(solution)/shard_map/ppermute | solution.py:145
  73.5 3.1 %collective-permute-start.11 = (bf16[1056,128]{1,0:T(8,128)(2,1)S(1)}, bf16[1056,128]{1,0:T(8,128)(2,1)S(1)}, u32[]{:S(2)}, u32[]{:S(2)}) collective-permute-start(bf16[1056,128]{1,0:T(8,128)(2,1)S(1)} %collective-permute-done.10), channel_id=1, source_target_pairs={{0,16},{1,241},{2,18},{3,243},{4,20},{5,245},{6,22},{7,247},{8,24}... | collective-permute-start | bytes 811016 | tf_op jit(solution)/shard_map/ppermute | solution.py:145
  76.6 2.0 collective-permute-start.3
  78.6 0.5 convolution_add_fusion.10
  79.1 4.8 %collective-permute-done.3 = bf16[1056,128]{1,0:T(8,128)(2,1)S(1)} collective-permute-done((bf16[1056,128]{1,0:T(8,128)(2,1)S(1)}, bf16[1056,128]{1,0:T(8,128)(2,1)S(1)}, u32[]{:S(2)}, u32[]{:S(2)}) %collective-permute-start.3) | collective-permute-done | bytes 270368 | tf_op jit(solution)/shard_map/ppermute | solution.py:145
  83.9 4.1 %collective-permute-start.4 = (bf16[704,128]{1,0:T(8,128)(2,1)S(1)}, bf16[704,128]{1,0:T(8,128)(2,1)S(1)}, u32[]{:S(2)}, u32[]{:S(2)}) collective-permute-start(bf16[704,128]{1,0:T(8,128)(2,1)S(1)} %slice.107), channel_id=1, source_target_pairs={{0,16},{1,241},{2,18},{3,243},{4,20},{5,245},{6,22},{7,247},{8,24}... | collective-permute-start | bytes 540680 | tf_op jit(solution)/shard_map/ppermute | solution.py:145
  88.0 0.5 convolution_add_fusion.4
  88.5 2.0 collective-permute-start.12
  90.5 5.0 %collective-permute-start.5 = (bf16[704,128]{1,0:T(8,128)(2,1)S(1)}, bf16[704,128]{1,0:T(8,128)(2,1)S(1)}, u32[]{:S(2)}, u32[]{:S(2)}) collective-permute-start(bf16[704,128]{1,0:T(8,128)(2,1)S(1)} %collective-permute-done.4), channel_id=1, source_target_pairs={{0,16},{1,241},{2,18},{3,243},{4,20},{5,245},{6,22},{7,247},{8,24}... | collective-permute-start | bytes 540680 | tf_op jit(solution)/shard_map/ppermute | solution.py:145
  95.9 0.5 fusion.19
  96.4 2.0 collective-permute-start.13
  98.4 0.5 fusion.1
  98.9 0.5 fusion
  99.3 3.6 %collective-permute-start.6 = (bf16[704,128]{1,0:T(8,128)(2,1)S(1)}, bf16[704,128]{1,0:T(8,128)(2,1)S(1)}, u32[]{:S(2)}, u32[]{:S(2)}) collective-permute-start(bf16[704,128]{1,0:T(8,128)(2,1)S(1)} %collective-permute-done.5), channel_id=1, source_target_pairs={{0,16},{1,241},{2,18},{3,243},{4,20},{5,245},{6,22},{7,247},{8,24}... | collective-permute-start | bytes 540680 | tf_op jit(solution)/shard_map/ppermute | solution.py:145
  102.9 2.9 %collective-permute-start.14 = (bf16[704,128]{1,0:T(8,128)(2,1)S(1)}, bf16[704,128]{1,0:T(8,128)(2,1)S(1)}, u32[]{:S(2)}, u32[]{:S(2)}) collective-permute-start(bf16[704,128]{1,0:T(8,128)(2,1)S(1)} %collective-permute-done.13), channel_id=1, source_target_pairs={{0,16},{1,241},{2,18},{3,243},{4,20},{5,245},{6,22},{7,247},{8,24}... | collective-permute-start | bytes 540680 | tf_op jit(solution)/shard_map/ppermute | solution.py:145
  105.9 0.5 convolution_add_fusion.8
  106.8 3.6 %collective-permute-start.7 = (bf16[704,128]{1,0:T(8,128)(2,1)S(1)}, bf16[704,128]{1,0:T(8,128)(2,1)S(1)}, u32[]{:S(2)}, u32[]{:S(2)}) collective-permute-start(bf16[704,128]{1,0:T(8,128)(2,1)S(1)} %collective-permute-done.6), channel_id=1, source_target_pairs={{0,16},{1,241},{2,18},{3,243},{4,20},{5,245},{6,22},{7,247},{8,24}... | collective-permute-start | bytes 540680 | tf_op jit(solution)/shard_map/ppermute | solution.py:145
  110.4 2.9 %collective-permute-start.15 = (bf16[704,128]{1,0:T(8,128)(2,1)S(1)}, bf16[704,128]{1,0:T(8,128)(2,1)S(1)}, u32[]{:S(2)}, u32[]{:S(2)}) collective-permute-start(bf16[704,128]{1,0:T(8,128)(2,1)S(1)} %collective-permute-done.14), channel_id=1, source_target_pairs={{0,16},{1,241},{2,18},{3,243},{4,20},{5,245},{6,22},{7,247},{8,24}... | collective-permute-start | bytes 540680 | tf_op jit(solution)/shard_map/ppermute | solution.py:145
  113.3 0.5 convolution_add_fusion.7
  114.3 0.5 fusion.42
  114.7 2.1 collective-permute-done.15
  117.4 5.3 %collective-permute-start.16 = (bf16[1408,512]{1,0:T(8,128)(2,1)S(1)}, bf16[1408,512]{1,0:T(8,128)(2,1)S(1)}, u32[]{:S(2)}, u32[]{:S(2)}) collective-permute-start(bf16[1408,512]{1,0:T(8,128)(2,1)S(1)} %pad_maximum_fusion), channel_id=1, source_target_pairs={{0,1},{1,0},{2,3},{3,2},{4,5},{5,4},{6,7},{7,6},{8,9},{9,8},{10,11... | collective-permute-start | bytes 4325384 | tf_op jit(solution)/shard_map/ppermute | solution.py:152
  123.1 2.7 %collective-permute-start.17 = (bf16[704,128]{1,0:T(8,128)(2,1)S(1)}, bf16[704,128]{1,0:T(8,128)(2,1)S(1)}, u32[]{:S(2)}, u32[]{:S(2)}) collective-permute-start(bf16[704,128]{1,0:T(8,128)(2,1)S(1)} %get-tuple-element.7), channel_id=1, source_target_pairs={{0,16},{1,241},{2,18},{3,243},{4,20},{5,245},{6,22},{7,247},{8,24}... | collective-permute-start | bytes 540680 | tf_op jit(solution)/shard_map/ppermute | solution.py:145
  125.8 3.8 %collective-permute-done.17 = bf16[704,128]{1,0:T(8,128)(2,1)S(1)} collective-permute-done((bf16[704,128]{1,0:T(8,128)(2,1)S(1)}, bf16[704,128]{1,0:T(8,128)(2,1)S(1)}, u32[]{:S(2)}, u32[]{:S(2)}) %collective-permute-start.17) | collective-permute-done | bytes 180256 | tf_op jit(solution)/shard_map/ppermute | solution.py:145
  129.6 3.6 %collective-permute-start.18 = (bf16[704,128]{1,0:T(8,128)(2,1)S(1)}, bf16[704,128]{1,0:T(8,128)(2,1)S(1)}, u32[]{:S(2)}, u32[]{:S(2)}) collective-permute-start(bf16[704,128]{1,0:T(8,128)(2,1)S(1)} %collective-permute-done.17), channel_id=1, source_target_pairs={{0,16},{1,241},{2,18},{3,243},{4,20},{5,245},{6,22},{7,247},{8,24}... | collective-permute-start | bytes 540680 | tf_op jit(solution)/shard_map/ppermute | solution.py:145
  133.2 2.6 %collective-permute-done.18 = bf16[704,128]{1,0:T(8,128)(2,1)S(1)} collective-permute-done((bf16[704,128]{1,0:T(8,128)(2,1)S(1)}, bf16[704,128]{1,0:T(8,128)(2,1)S(1)}, u32[]{:S(2)}, u32[]{:S(2)}) %collective-permute-start.18) | collective-permute-done | bytes 180256 | tf_op jit(solution)/shard_map/ppermute | solution.py:145
  135.9 4.8 %collective-permute-start.19 = (bf16[704,128]{1,0:T(8,128)(2,1)S(1)}, bf16[704,128]{1,0:T(8,128)(2,1)S(1)}, u32[]{:S(2)}, u32[]{:S(2)}) collective-permute-start(bf16[704,128]{1,0:T(8,128)(2,1)S(1)} %collective-permute-done.18), channel_id=1, source_target_pairs={{0,16},{1,241},{2,18},{3,243},{4,20},{5,245},{6,22},{7,247},{8,24}... | collective-permute-start | bytes 540680 | tf_op jit(solution)/shard_map/ppermute | solution.py:145
  140.8 2.4 %collective-permute-done.19 = bf16[704,128]{1,0:T(8,128)(2,1)S(1)} collective-permute-done((bf16[704,128]{1,0:T(8,128)(2,1)S(1)}, bf16[704,128]{1,0:T(8,128)(2,1)S(1)}, u32[]{:S(2)}, u32[]{:S(2)}) %collective-permute-start.19) | collective-permute-done | bytes 180256 | tf_op jit(solution)/shard_map/ppermute | solution.py:145
  143.1 5.0 %collective-permute-start.20 = (bf16[704,128]{1,0:T(8,128)(2,1)S(1)}, bf16[704,128]{1,0:T(8,128)(2,1)S(1)}, u32[]{:S(2)}, u32[]{:S(2)}) collective-permute-start(bf16[704,128]{1,0:T(8,128)(2,1)S(1)} %collective-permute-done.19), channel_id=1, source_target_pairs={{0,16},{1,241},{2,18},{3,243},{4,20},{5,245},{6,22},{7,247},{8,24}... | collective-permute-start | bytes 540680 | tf_op jit(solution)/shard_map/ppermute | solution.py:145
  148.3 2.3 %collective-permute-done.20 = bf16[704,128]{1,0:T(8,128)(2,1)S(1)} collective-permute-done((bf16[704,128]{1,0:T(8,128)(2,1)S(1)}, bf16[704,128]{1,0:T(8,128)(2,1)S(1)}, u32[]{:S(2)}, u32[]{:S(2)}) %collective-permute-start.20) | collective-permute-done | bytes 180256 | tf_op jit(solution)/shard_map/ppermute | solution.py:145
  150.7 0.6 fusion.5
  151.2 1.0 convolution_convert_fusion
  152.2 27.7 %all_to_all.10 = bf16[8,64,1024]{2,1,0:T(8,128)(2,1)S(1)} all-to-all(bf16[8,64,1024]{2,1,0:T(8,128)(2,1)S(1)} %bitcast.23), channel_id=1, replica_groups={{0,2,4,6,8,10,12,14},{1,3,5,7,9,11,13,15},{16,18,20,22,24,26,28,30},{17..., dimensions={0} | all-to-all | bytes 2097152 | tf_op jit(solution)/shard_map/all_to_all | solution.py:170
  180.3 23.8 %all_to_all.11 = bf16[8,64,1024]{2,1,0:T(8,128)(2,1)S(1)} all-to-all(bf16[8,64,1024]{2,1,0:T(8,128)(2,1)S(1)} %broadcast_in_dim.2), channel_id=1, replica_groups={{0,2,4,6,8,10,12,14},{1,3,5,7,9,11,13,15},{16,18,20,22,24,26,28,30},{17..., dimensions={0} | all-to-all | bytes 2097152 | tf_op jit(solution)/shard_map/all_to_all | solution.py:170
  204.1 11.4 %collective-permute-start.21 = (bf16[512,1024]{1,0:T(8,128)(2,1)S(1)}, bf16[512,1024]{1,0:T(8,128)(2,1)S(1)}, u32[]{:S(2)}, u32[]{:S(2)}) collective-permute-start(bf16[512,1024]{1,0:T(8,128)(2,1)S(1)} %bitcast.19), channel_id=1, source_target_pairs={{0,1},{1,0},{2,3},{3,2},{4,5},{5,4},{6,7},{7,6},{8,9},{9,8},{10,11... | collective-permute-start | bytes 3145736 | tf_op jit(solution)/shard_map/ppermute | solution.py:187
  215.5 2.2 collective-permute-done.21.refs_2_
  217.7 2.9 %shard_map.91 = bf16[512,2048]{1,0:T(8,128)(2,1)} custom-call(s32[2]{0:T(128)S(1)} %pad_add_fusion.refs_0_, bf16[512,1024]{1,0:T(8,128)(2,1)S(1)} %bitcast.20, bf16[512,1024]{1,0:T(8,128)(2,1)S(1)} %collective-permute-done.21.refs_2_, f32[16,128]{1,0:T(8,128)S(1)} %bitcast.21, f32[16,128]{1,0:T(8,128)S(1)} %bitcast.22), custom_call_target="tpu_custom_call" | custom-call | tf_op jit(solution)/shard_map/pallas_call | solution.py:72
  (54 shorter events, 4.9 us)
Async XLA Ops:
  2.2 54.7 %copy-start.3 = (f32[2048]{0:T(1024)S(1)}, f32[2048]{0:T(1024)}, u32[]{:S(2)}) copy-start(f32[2048]{0:T(1024)} %param.10) | copy-start | bytes 24580
  2.2 56.8 %copy-start.2 = (bf16[512,2048]{1,0:T(8,128)(2,1)S(1)}, bf16[512,2048]{1,0:T(8,128)(2,1)}, u32[]{:S(2)}) copy-start(bf16[512,2048]{1,0:T(8,128)(2,1)} %param.9) | copy-start | bytes 6291460
  2.2 54.8 %collective-permute-start.8 = (bf16[1056,128]{1,0:T(8,128)(2,1)S(1)}, bf16[1056,128]{1,0:T(8,128)(2,1)S(1)}, u32[]{:S(2)}, u32[]{:S(2)}) collective-permute-start(bf16[1056,128]{1,0:T(8,128)(2,1)S(1)} %pad_maximum_fusion.1), channel_id=1, source_target_pairs={{0,241},{1,0},{2,243},{3,2},{4,245},{5,4},{6,247},{7,6},{8,249},{9... | collective-permute-start | bytes 811016 | tf_op jit(solution)/shard_map/ppermute | solution.py:116
  43.7 8.1 %collective-permute-start = (bf16[1056,128]{1,0:T(8,128)(2,1)S(1)}, bf16[1056,128]{1,0:T(8,128)(2,1)S(1)}, u32[]{:S(2)}, u32[]{:S(2)}) collective-permute-start(bf16[1056,128]{1,0:T(8,128)(2,1)S(1)} %pad_maximum_fusion.1), channel_id=1, source_target_pairs={{1,241},{3,243},{5,245},{7,247},{9,249},{11,251},{13,253},{15,255}... | collective-permute-start | bytes 811016 | tf_op jit(solution)/shard_map/ppermute | solution.py:117
  51.8 8.4 %collective-permute-start.1 = (bf16[1056,128]{1,0:T(8,128)(2,1)S(1)}, bf16[1056,128]{1,0:T(8,128)(2,1)S(1)}, u32[]{:S(2)}, u32[]{:S(2)}) collective-permute-start(bf16[1056,128]{1,0:T(8,128)(2,1)S(1)} %broadcast_select_fusion), channel_id=1, source_target_pairs={{0,16},{1,241},{2,18},{3,243},{4,20},{5,245},{6,22},{7,247},{8,24}... | collective-permute-start | bytes 811016 | tf_op jit(solution)/shard_map/ppermute | solution.py:145
  57.0 9.2 %collective-permute-start.9 = (bf16[1056,128]{1,0:T(8,128)(2,1)S(1)}, bf16[1056,128]{1,0:T(8,128)(2,1)S(1)}, u32[]{:S(2)}, u32[]{:S(2)}) collective-permute-start(bf16[1056,128]{1,0:T(8,128)(2,1)S(1)} %collective-permute-done.8), channel_id=1, source_target_pairs={{0,16},{1,241},{2,18},{3,243},{4,20},{5,245},{6,22},{7,247},{8,24}... | collective-permute-start | bytes 811016 | tf_op jit(solution)/shard_map/ppermute | solution.py:145
  60.3 16.4 %collective-permute-start.2 = (bf16[1056,128]{1,0:T(8,128)(2,1)S(1)}, bf16[1056,128]{1,0:T(8,128)(2,1)S(1)}, u32[]{:S(2)}, u32[]{:S(2)}) collective-permute-start(bf16[1056,128]{1,0:T(8,128)(2,1)S(1)} %collective-permute-done.1), channel_id=1, source_target_pairs={{0,16},{1,241},{2,18},{3,243},{4,20},{5,245},{6,22},{7,247},{8,24}... | collective-permute-start | bytes 811016 | tf_op jit(solution)/shard_map/ppermute | solution.py:145
  66.2 7.2 %collective-permute-start.10 = (bf16[1056,128]{1,0:T(8,128)(2,1)S(1)}, bf16[1056,128]{1,0:T(8,128)(2,1)S(1)}, u32[]{:S(2)}, u32[]{:S(2)}) collective-permute-start(bf16[1056,128]{1,0:T(8,128)(2,1)S(1)} %collective-permute-done.9), channel_id=1, source_target_pairs={{0,16},{1,241},{2,18},{3,243},{4,20},{5,245},{6,22},{7,247},{8,24}... | collective-permute-start | bytes 811016 | tf_op jit(solution)/shard_map/ppermute | solution.py:145
  73.5 15.0 %collective-permute-start.11 = (bf16[1056,128]{1,0:T(8,128)(2,1)S(1)}, bf16[1056,128]{1,0:T(8,128)(2,1)S(1)}, u32[]{:S(2)}, u32[]{:S(2)}) collective-permute-start(bf16[1056,128]{1,0:T(8,128)(2,1)S(1)} %collective-permute-done.10), channel_id=1, source_target_pairs={{0,16},{1,241},{2,18},{3,243},{4,20},{5,245},{6,22},{7,247},{8,24}... | collective-permute-start | bytes 811016 | tf_op jit(solution)/shard_map/ppermute | solution.py:145
  76.6 7.2 %collective-permute-start.3 = (bf16[1056,128]{1,0:T(8,128)(2,1)S(1)}, bf16[1056,128]{1,0:T(8,128)(2,1)S(1)}, u32[]{:S(2)}, u32[]{:S(2)}) collective-permute-start(bf16[1056,128]{1,0:T(8,128)(2,1)S(1)} %collective-permute-done.2), channel_id=1, source_target_pairs={{0,16},{1,241},{2,18},{3,243},{4,20},{5,245},{6,22},{7,247},{8,24}... | collective-permute-start | bytes 811016 | tf_op jit(solution)/shard_map/ppermute | solution.py:145
  83.9 6.6 %collective-permute-start.4 = (bf16[704,128]{1,0:T(8,128)(2,1)S(1)}, bf16[704,128]{1,0:T(8,128)(2,1)S(1)}, u32[]{:S(2)}, u32[]{:S(2)}) collective-permute-start(bf16[704,128]{1,0:T(8,128)(2,1)S(1)} %slice.107), channel_id=1, source_target_pairs={{0,16},{1,241},{2,18},{3,243},{4,20},{5,245},{6,22},{7,247},{8,24}... | collective-permute-start | bytes 540680 | tf_op jit(solution)/shard_map/ppermute | solution.py:145
  88.5 7.4 %collective-permute-start.12 = (bf16[704,128]{1,0:T(8,128)(2,1)S(1)}, bf16[704,128]{1,0:T(8,128)(2,1)S(1)}, u32[]{:S(2)}, u32[]{:S(2)}) collective-permute-start(bf16[704,128]{1,0:T(8,128)(2,1)S(1)} %slice.112), channel_id=1, source_target_pairs={{0,16},{1,241},{2,18},{3,243},{4,20},{5,245},{6,22},{7,247},{8,24}... | collective-permute-start | bytes 540680 | tf_op jit(solution)/shard_map/ppermute | solution.py:145
  90.5 8.9 %collective-permute-start.5 = (bf16[704,128]{1,0:T(8,128)(2,1)S(1)}, bf16[704,128]{1,0:T(8,128)(2,1)S(1)}, u32[]{:S(2)}, u32[]{:S(2)}) collective-permute-start(bf16[704,128]{1,0:T(8,128)(2,1)S(1)} %collective-permute-done.4), channel_id=1, source_target_pairs={{0,16},{1,241},{2,18},{3,243},{4,20},{5,245},{6,22},{7,247},{8,24}... | collective-permute-start | bytes 540680 | tf_op jit(solution)/shard_map/ppermute | solution.py:145
  96.4 6.5 %collective-permute-start.13 = (bf16[704,128]{1,0:T(8,128)(2,1)S(1)}, bf16[704,128]{1,0:T(8,128)(2,1)S(1)}, u32[]{:S(2)}, u32[]{:S(2)}) collective-permute-start(bf16[704,128]{1,0:T(8,128)(2,1)S(1)} %collective-permute-done.12), channel_id=1, source_target_pairs={{0,16},{1,241},{2,18},{3,243},{4,20},{5,245},{6,22},{7,247},{8,24}... | collective-permute-start | bytes 540680 | tf_op jit(solution)/shard_map/ppermute | solution.py:145
  99.3 7.5 %collective-permute-start.6 = (bf16[704,128]{1,0:T(8,128)(2,1)S(1)}, bf16[704,128]{1,0:T(8,128)(2,1)S(1)}, u32[]{:S(2)}, u32[]{:S(2)}) collective-permute-start(bf16[704,128]{1,0:T(8,128)(2,1)S(1)} %collective-permute-done.5), channel_id=1, source_target_pairs={{0,16},{1,241},{2,18},{3,243},{4,20},{5,245},{6,22},{7,247},{8,24}... | collective-permute-start | bytes 540680 | tf_op jit(solution)/shard_map/ppermute | solution.py:145
  102.9 7.5 %collective-permute-start.14 = (bf16[704,128]{1,0:T(8,128)(2,1)S(1)}, bf16[704,128]{1,0:T(8,128)(2,1)S(1)}, u32[]{:S(2)}, u32[]{:S(2)}) collective-permute-start(bf16[704,128]{1,0:T(8,128)(2,1)S(1)} %collective-permute-done.13), channel_id=1, source_target_pairs={{0,16},{1,241},{2,18},{3,243},{4,20},{5,245},{6,22},{7,247},{8,24}... | collective-permute-start | bytes 540680 | tf_op jit(solution)/shard_map/ppermute | solution.py:145
  106.8 7.5 %collective-permute-start.7 = (bf16[704,128]{1,0:T(8,128)(2,1)S(1)}, bf16[704,128]{1,0:T(8,128)(2,1)S(1)}, u32[]{:S(2)}, u32[]{:S(2)}) collective-permute-start(bf16[704,128]{1,0:T(8,128)(2,1)S(1)} %collective-permute-done.6), channel_id=1, source_target_pairs={{0,16},{1,241},{2,18},{3,243},{4,20},{5,245},{6,22},{7,247},{8,24}... | collective-permute-start | bytes 540680 | tf_op jit(solution)/shard_map/ppermute | solution.py:145
  110.4 6.4 %collective-permute-start.15 = (bf16[704,128]{1,0:T(8,128)(2,1)S(1)}, bf16[704,128]{1,0:T(8,128)(2,1)S(1)}, u32[]{:S(2)}, u32[]{:S(2)}) collective-permute-start(bf16[704,128]{1,0:T(8,128)(2,1)S(1)} %collective-permute-done.14), channel_id=1, source_target_pairs={{0,16},{1,241},{2,18},{3,243},{4,20},{5,245},{6,22},{7,247},{8,24}... | collective-permute-start | bytes 540680 | tf_op jit(solution)/shard_map/ppermute | solution.py:145
  117.4 33.3 %collective-permute-start.16 = (bf16[1408,512]{1,0:T(8,128)(2,1)S(1)}, bf16[1408,512]{1,0:T(8,128)(2,1)S(1)}, u32[]{:S(2)}, u32[]{:S(2)}) collective-permute-start(bf16[1408,512]{1,0:T(8,128)(2,1)S(1)} %pad_maximum_fusion), channel_id=1, source_target_pairs={{0,1},{1,0},{2,3},{3,2},{4,5},{5,4},{6,7},{7,6},{8,9},{9,8},{10,11... | collective-permute-start | bytes 4325384 | tf_op jit(solution)/shard_map/ppermute | solution.py:152
  123.1 6.6 %collective-permute-start.17 = (bf16[704,128]{1,0:T(8,128)(2,1)S(1)}, bf16[704,128]{1,0:T(8,128)(2,1)S(1)}, u32[]{:S(2)}, u32[]{:S(2)}) collective-permute-start(bf16[704,128]{1,0:T(8,128)(2,1)S(1)} %get-tuple-element.7), channel_id=1, source_target_pairs={{0,16},{1,241},{2,18},{3,243},{4,20},{5,245},{6,22},{7,247},{8,24}... | collective-permute-start | bytes 540680 | tf_op jit(solution)/shard_map/ppermute | solution.py:145
  129.6 6.3 %collective-permute-start.18 = (bf16[704,128]{1,0:T(8,128)(2,1)S(1)}, bf16[704,128]{1,0:T(8,128)(2,1)S(1)}, u32[]{:S(2)}, u32[]{:S(2)}) collective-permute-start(bf16[704,128]{1,0:T(8,128)(2,1)S(1)} %collective-permute-done.17), channel_id=1, source_target_pairs={{0,16},{1,241},{2,18},{3,243},{4,20},{5,245},{6,22},{7,247},{8,24}... | collective-permute-start | bytes 540680 | tf_op jit(solution)/shard_map/ppermute | solution.py:145
  135.9 7.2 %collective-permute-start.19 = (bf16[704,128]{1,0:T(8,128)(2,1)S(1)}, bf16[704,128]{1,0:T(8,128)(2,1)S(1)}, u32[]{:S(2)}, u32[]{:S(2)}) collective-permute-start(bf16[704,128]{1,0:T(8,128)(2,1)S(1)} %collective-permute-done.18), channel_id=1, source_target_pairs={{0,16},{1,241},{2,18},{3,243},{4,20},{5,245},{6,22},{7,247},{8,24}... | collective-permute-start | bytes 540680 | tf_op jit(solution)/shard_map/ppermute | solution.py:145
  143.1 7.5 %collective-permute-start.20 = (bf16[704,128]{1,0:T(8,128)(2,1)S(1)}, bf16[704,128]{1,0:T(8,128)(2,1)S(1)}, u32[]{:S(2)}, u32[]{:S(2)}) collective-permute-start(bf16[704,128]{1,0:T(8,128)(2,1)S(1)} %collective-permute-done.19), channel_id=1, source_target_pairs={{0,16},{1,241},{2,18},{3,243},{4,20},{5,245},{6,22},{7,247},{8,24}... | collective-permute-start | bytes 540680 | tf_op jit(solution)/shard_map/ppermute | solution.py:145
  180.2 37.6 %copy-start = (f32[2048]{0:T(1024)S(1)}, f32[2048]{0:T(1024)}, u32[]{:S(2)}) copy-start(f32[2048]{0:T(1024)} %param.16) | copy-start | bytes 24580
  180.2 37.6 %copy-start.1 = (f32[2048]{0:T(1024)S(1)}, f32[2048]{0:T(1024)}, u32[]{:S(2)}) copy-start(f32[2048]{0:T(1024)} %param.17) | copy-start | bytes 24580
  204.1 13.7 %collective-permute-start.21 = (bf16[512,1024]{1,0:T(8,128)(2,1)S(1)}, bf16[512,1024]{1,0:T(8,128)(2,1)S(1)}, u32[]{:S(2)}, u32[]{:S(2)}) collective-permute-start(bf16[512,1024]{1,0:T(8,128)(2,1)S(1)} %bitcast.19), channel_id=1, source_target_pairs={{0,1},{1,0},{2,3},{3,2},{4,5},{5,4},{6,7},{7,6},{8,9},{9,8},{10,11... | collective-permute-start | bytes 3145736 | tf_op jit(solution)/shard_map/ppermute | solution.py:187

commit v2 on v0

--- a/solution.py
+++ b/solution.py
@@ -142,16 +142,15 @@
         sum_own = sum_own + product(held["own"][: 2 * units], slab)
         sum_other = sum_other + product(held["other"][: 2 * units], slab)
 
-    sums = jnp.concatenate([sum_own, sum_other], axis=0).astype(low)
-    arrived = lax.ppermute(sums, "tp", partner)
+    for_other = lax.ppermute(sum_own.astype(low), "tp", partner)
+    for_own = lax.ppermute(sum_other.astype(low), "tp", partner)
 
     def gated(sums, more):
-        sums = sums + more.astype(jnp.float32)
-        return (jax.nn.silu(sums[:units]) * sums[units:]).astype(low)
+        gate = sums[:units] + more[:units].astype(jnp.float32)
+        up = sums[units:] + more[units:].astype(jnp.float32)
+        return (jax.nn.silu(gate) * up).astype(low)
 
-    hidden = jnp.concatenate(
-        [gated(sum_own, arrived[2 * units :]), gated(sum_other, arrived[: 2 * units])], axis=0
-    )
+    hidden = jnp.concatenate([gated(sum_own, for_own), gated(sum_other, for_other)], axis=0)
     columns = jnp.concatenate(downs, axis=1)
 
     n_rows = tokens.shape[0]

time: 204 us -> 212 us (1.039)
  waiting for transfers between devices: 17.3 us -> 22.8 us
  blocking collectives: 63.6 us -> 67 us
    ppermute x14, waiting for transfers between devices: 10.8 us -> 17.3 us  [body(): held[chain] = lax.ppermute(held[chain], both, ring)]
    all_to_all x2, blocking collectives: 63.6 us -> 67 us  [over_chips(): lax.all_to_all(array, 'tp', 0, 0, axis_index_groups=chips, tiled=True)]
    ppermute x1 -> x2, starting transfers between devices: 5.11 us -> 7.37 us  [the longest x1 5.42 us: body(): for_other = lax.ppermute(sum_own.astype(low), 'tp', partner)]
    ppermute x1, starting transfers between devices: 5.25 us -> 3.06 us  [body(): other = lax.ppermute(mine, 'tp', partner)]
  transfers between devices with their start and end apart: 18 -> 19, of which waited for: 7 -> 11; matrix products, arithmetic and copies ran while one was open for 5% -> 5% of each run, Pallas kernels for 0% -> 0%
where the time goes in v2:
time: 212 us; the launch traced here: 211 us
  starting transfers between devices  104 us (49%)
  blocking collectives  67 us (32%)
  waiting for transfers between devices  22.8 us (11%)
  matrix products  8.32 us (4%)
  other arithmetic  5.68 us (3%)
  Pallas kernels  2.95 us (1%)
    all_to_all x2, blocking collectives, over_chips(): lax.all_to_all(array, 'tp', 0, 0, axis_index_groups=chips, tiled=True)  67 us
    ppermute x14, starting transfers between devices, body(): held[chain] = lax.ppermute(held[chain], both, ring)  47.9 us
    ppermute x1, starting transfers between devices, body(): other0 = lax.ppermute(packed, both, enter)  41.5 us
    ppermute x14, waiting for transfers between devices, body(): held[chain] = lax.ppermute(held[chain], both, ring)  17.3 us
    dot_general x16, matrix products, product(): lax.dot_general(weights, k_normed, (((1,), (1,)), ((), ())), preferred_el...  7.31 us
    ppermute x1, starting transfers between devices, body(): for_other = lax.ppermute(sum_own.astype(low), 'tp', partner)  5.42 us
  transfers between devices with their start and end apart: 19, of which 11 were waited for; matrix products, arithmetic and copies ran while one was open for 5% of the time, Pallas kernels for 0%

profile of v2, /device:TPU:65, one launch (start us, length us, event | category | flops | bytes accessed | tf_op | source)
XLA Modules:
  0.0 211.3 jit_solution(5136486848559754792)
XLA Ops:
  0.0 0.9 convert_element_type.91
  0.9 1.2 fusion.25
  2.2 41.5 %collective-permute-start.8 = (bf16[1056,128]{1,0:T(8,128)(2,1)S(1)}, bf16[1056,128]{1,0:T(8,128)(2,1)S(1)}, u32[]{:S(2)}, u32[]{:S(2)}) collective-permute-start(bf16[1056,128]{1,0:T(8,128)(2,1)S(1)} %pad_maximum_fusion), channel_id=1, source_target_pairs={{0,241},{1,0},{2,243},{3,2},{4,245},{5,4},{6,247},{7,6},{8,249},{9... | collective-permute-start | bytes 811016 | tf_op jit(solution)/shard_map/ppermute | solution.py:112
  43.6 3.7 %collective-permute-start = (bf16[1056,128]{1,0:T(8,128)(2,1)S(1)}, bf16[1056,128]{1,0:T(8,128)(2,1)S(1)}, u32[]{:S(2)}, u32[]{:S(2)}) collective-permute-start(bf16[1056,128]{1,0:T(8,128)(2,1)S(1)} %pad_maximum_fusion), channel_id=1, source_target_pairs={{1,241},{3,243},{5,245},{7,247},{9,249},{11,251},{13,253},{15,255}... | collective-permute-start | bytes 811016 | tf_op jit(solution)/shard_map/ppermute | solution.py:113
  47.5 2.2 %multiply_reduce_fusion = f32[512]{0:T(512)S(1)} fusion(bf16[512,2048]{1,0:T(8,128)(2,1)} %param.9), kind=kLoop, calls=%fused_computation | loop fusion | flops 3145216 | bytes 2099200 | tf_op jit(solution)/shard_map/reduce_sum | solution.py:117
  49.9 1.8 collective-permute-done
  51.8 5.1 %collective-permute-start.1 = (bf16[1056,128]{1,0:T(8,128)(2,1)S(1)}, bf16[1056,128]{1,0:T(8,128)(2,1)S(1)}, u32[]{:S(2)}, u32[]{:S(2)}) collective-permute-start(bf16[1056,128]{1,0:T(8,128)(2,1)S(1)} %broadcast_select_fusion), channel_id=1, source_target_pairs={{0,16},{1,241},{2,18},{3,243},{4,20},{5,245},{6,22},{7,247},{8,24}... | collective-permute-start | bytes 811016 | tf_op jit(solution)/shard_map/ppermute | solution.py:139
  57.0 2.0 collective-permute-start.9
  58.9 0.5 fusion.14
  59.4 0.9 collective-permute-done.1
  60.7 0.5 convolution_add_fusion.13
  61.2 3.0 %collective-permute-done.9 = bf16[1056,128]{1,0:T(8,128)(2,1)S(1)} collective-permute-done((bf16[1056,128]{1,0:T(8,128)(2,1)S(1)}, bf16[1056,128]{1,0:T(8,128)(2,1)S(1)}, u32[]{:S(2)}, u32[]{:S(2)}) %collective-permute-start.9) | collective-permute-done | bytes 270368 | tf_op jit(solution)/shard_map/ppermute | solution.py:139
  64.3 4.0 %collective-permute-start.10 = (bf16[1056,128]{1,0:T(8,128)(2,1)S(1)}, bf16[1056,128]{1,0:T(8,128)(2,1)S(1)}, u32[]{:S(2)}, u32[]{:S(2)}) collective-permute-start(bf16[1056,128]{1,0:T(8,128)(2,1)S(1)} %collective-permute-done.9), channel_id=1, source_target_pairs={{0,16},{1,241},{2,18},{3,243},{4,20},{5,245},{6,22},{7,247},{8,24}... | collective-permute-start | bytes 811016 | tf_op jit(solution)/shard_map/ppermute | solution.py:139
  68.3 2.0 collective-permute-start.2
  70.2 0.5 convolution_add_fusion.6
  70.7 1.1 collective-permute-done.10
  71.8 3.7 %collective-permute-done.2 = bf16[1056,128]{1,0:T(8,128)(2,1)S(1)} collective-permute-done((bf16[1056,128]{1,0:T(8,128)(2,1)S(1)}, bf16[1056,128]{1,0:T(8,128)(2,1)S(1)}, u32[]{:S(2)}, u32[]{:S(2)}) %collective-permute-start.2) | collective-permute-done | bytes 270368 | tf_op jit(solution)/shard_map/ppermute | solution.py:139
  75.6 4.1 %collective-permute-start.11 = (bf16[1056,128]{1,0:T(8,128)(2,1)S(1)}, bf16[1056,128]{1,0:T(8,128)(2,1)S(1)}, u32[]{:S(2)}, u32[]{:S(2)}) collective-permute-start(bf16[1056,128]{1,0:T(8,128)(2,1)S(1)} %collective-permute-done.10), channel_id=1, source_target_pairs={{0,16},{1,241},{2,18},{3,243},{4,20},{5,245},{6,22},{7,247},{8,24}... | collective-permute-start | bytes 811016 | tf_op jit(solution)/shard_map/ppermute | solution.py:139
  79.7 2.0 collective-permute-start.3
  81.7 0.5 convolution_add_fusion.5
  82.1 0.5 convolution_add_fusion.12
  82.6 0.5 collective-permute-done.11
  83.1 3.8 %collective-permute-done.3 = bf16[1056,128]{1,0:T(8,128)(2,1)S(1)} collective-permute-done((bf16[1056,128]{1,0:T(8,128)(2,1)S(1)}, bf16[1056,128]{1,0:T(8,128)(2,1)S(1)}, u32[]{:S(2)}, u32[]{:S(2)}) %collective-permute-start.3) | collective-permute-done | bytes 270368 | tf_op jit(solution)/shard_map/ppermute | solution.py:139
  87.0 4.1 %collective-permute-start.12 = (bf16[1056,128]{1,0:T(8,128)(2,1)S(1)}, bf16[1056,128]{1,0:T(8,128)(2,1)S(1)}, u32[]{:S(2)}, u32[]{:S(2)}) collective-permute-start(bf16[1056,128]{1,0:T(8,128)(2,1)S(1)} %collective-permute-done.11), channel_id=1, source_target_pairs={{0,16},{1,241},{2,18},{3,243},{4,20},{5,245},{6,22},{7,247},{8,24}... | collective-permute-start | bytes 811016 | tf_op jit(solution)/shard_map/ppermute | solution.py:139
  91.1 2.0 collective-permute-start.4
  93.1 0.5 convolution_add_fusion.4
  93.5 0.5 convolution_add_fusion.11
  94.0 0.5 collective-permute-done.12
  94.5 5.0 %collective-permute-start.13 = (bf16[1056,128]{1,0:T(8,128)(2,1)S(1)}, bf16[1056,128]{1,0:T(8,128)(2,1)S(1)}, u32[]{:S(2)}, u32[]{:S(2)}) collective-permute-start(bf16[1056,128]{1,0:T(8,128)(2,1)S(1)} %collective-permute-done.12), channel_id=1, source_target_pairs={{0,16},{1,241},{2,18},{3,243},{4,20},{5,245},{6,22},{7,247},{8,24}... | collective-permute-start | bytes 811016 | tf_op jit(solution)/shard_map/ppermute | solution.py:139
  99.6 2.9 %collective-permute-start.5 = (bf16[1056,128]{1,0:T(8,128)(2,1)S(1)}, bf16[1056,128]{1,0:T(8,128)(2,1)S(1)}, u32[]{:S(2)}, u32[]{:S(2)}) collective-permute-start(bf16[1056,128]{1,0:T(8,128)(2,1)S(1)} %collective-permute-done.4), channel_id=1, source_target_pairs={{0,16},{1,241},{2,18},{3,243},{4,20},{5,245},{6,22},{7,247},{8,24}... | collective-permute-start | bytes 811016 | tf_op jit(solution)/shard_map/ppermute | solution.py:139
  102.5 0.5 convolution_add_fusion.3
  103.4 4.6 %collective-permute-start.14 = (bf16[1056,128]{1,0:T(8,128)(2,1)S(1)}, bf16[1056,128]{1,0:T(8,128)(2,1)S(1)}, u32[]{:S(2)}, u32[]{:S(2)}) collective-permute-start(bf16[1056,128]{1,0:T(8,128)(2,1)S(1)} %collective-permute-done.13), channel_id=1, source_target_pairs={{0,16},{1,241},{2,18},{3,243},{4,20},{5,245},{6,22},{7,247},{8,24}... | collective-permute-start | bytes 811016 | tf_op jit(solution)/shard_map/ppermute | solution.py:139
  108.0 2.9 %collective-permute-start.6 = (bf16[1056,128]{1,0:T(8,128)(2,1)S(1)}, bf16[1056,128]{1,0:T(8,128)(2,1)S(1)}, u32[]{:S(2)}, u32[]{:S(2)}) collective-permute-start(bf16[1056,128]{1,0:T(8,128)(2,1)S(1)} %collective-permute-done.5), channel_id=1, source_target_pairs={{0,16},{1,241},{2,18},{3,243},{4,20},{5,245},{6,22},{7,247},{8,24}... | collective-permute-start | bytes 811016 | tf_op jit(solution)/shard_map/ppermute | solution.py:139
  110.9 0.5 convolution_add_fusion.2
  111.4 0.5 convolution_add_fusion.9
  111.8 4.6 %collective-permute-start.15 = (bf16[1056,128]{1,0:T(8,128)(2,1)S(1)}, bf16[1056,128]{1,0:T(8,128)(2,1)S(1)}, u32[]{:S(2)}, u32[]{:S(2)}) collective-permute-start(bf16[1056,128]{1,0:T(8,128)(2,1)S(1)} %collective-permute-done.14), channel_id=1, source_target_pairs={{0,16},{1,241},{2,18},{3,243},{4,20},{5,245},{6,22},{7,247},{8,24}... | collective-permute-start | bytes 811016 | tf_op jit(solution)/shard_map/ppermute | solution.py:139
  116.4 2.9 %collective-permute-start.7 = (bf16[1056,128]{1,0:T(8,128)(2,1)S(1)}, bf16[1056,128]{1,0:T(8,128)(2,1)S(1)}, u32[]{:S(2)}, u32[]{:S(2)}) collective-permute-start(bf16[1056,128]{1,0:T(8,128)(2,1)S(1)} %collective-permute-done.6), channel_id=1, source_target_pairs={{0,16},{1,241},{2,18},{3,243},{4,20},{5,245},{6,22},{7,247},{8,24}... | collective-permute-start | bytes 811016 | tf_op jit(solution)/shard_map/ppermute | solution.py:139
  120.2 3.7 %collective-permute-done.7 = bf16[1056,128]{1,0:T(8,128)(2,1)S(1)} collective-permute-done((bf16[1056,128]{1,0:T(8,128)(2,1)S(1)}, bf16[1056,128]{1,0:T(8,128)(2,1)S(1)}, u32[]{:S(2)}, u32[]{:S(2)}) %collective-permute-start.7) | collective-permute-done | bytes 270368 | tf_op jit(solution)/shard_map/ppermute | solution.py:139
  124.4 5.4 %collective-permute-start.17 = (bf16[704,512]{1,0:T(8,128)(2,1)S(1)}, bf16[704,512]{1,0:T(8,128)(2,1)S(1)}, u32[]{:S(2)}, u32[]{:S(2)}) collective-permute-start(bf16[704,512]{1,0:T(8,128)(2,1)S(1)} %get-tuple-element.13), channel_id=1, source_target_pairs={{0,1},{1,0},{2,3},{3,2},{4,5},{5,4},{6,7},{7,6},{8,9},{9,8},{10,11... | collective-permute-start | bytes 2162696 | tf_op jit(solution)/shard_map/ppermute | solution.py:145
  129.9 0.5 fusion.46
  130.3 2.0 collective-permute-start.16
  132.9 1.5 collective-permute-done.16
  134.7 1.0 convolution_convert_fusion
  135.7 36.0 %all_to_all.10 = bf16[8,64,1024]{2,1,0:T(8,128)(2,1)S(1)} all-to-all(bf16[8,64,1024]{2,1,0:T(8,128)(2,1)S(1)} %bitcast.15), channel_id=1, replica_groups={{0,2,4,6,8,10,12,14},{1,3,5,7,9,11,13,15},{16,18,20,22,24,26,28,30},{17..., dimensions={0} | all-to-all | bytes 2097152 | tf_op jit(solution)/shard_map/all_to_all | solution.py:162
  172.0 31.0 %all_to_all.11 = bf16[8,64,1024]{2,1,0:T(8,128)(2,1)S(1)} all-to-all(bf16[8,64,1024]{2,1,0:T(8,128)(2,1)S(1)} %broadcast_in_dim.2), channel_id=1, replica_groups={{0,2,4,6,8,10,12,14},{1,3,5,7,9,11,13,15},{16,18,20,22,24,26,28,30},{17..., dimensions={0} | all-to-all | bytes 2097152 | tf_op jit(solution)/shard_map/all_to_all | solution.py:162
  203.0 3.1 %collective-permute-start.18 = (bf16[512,1024]{1,0:T(8,128)(2,1)S(1)}, bf16[512,1024]{1,0:T(8,128)(2,1)S(1)}, u32[]{:S(2)}, u32[]{:S(2)}) collective-permute-start(bf16[512,1024]{1,0:T(8,128)(2,1)S(1)} %bitcast.11), channel_id=1, source_target_pairs={{0,1},{1,0},{2,3},{3,2},{4,5},{5,4},{6,7},{7,6},{8,9},{9,8},{10,11... | collective-permute-start | bytes 3145736 | tf_op jit(solution)/shard_map/ppermute | solution.py:179
  206.2 2.2 %collective-permute-done.18.refs_2_ = bf16[512,1024]{1,0:T(8,128)(2,1)S(1)} collective-permute-done((bf16[512,1024]{1,0:T(8,128)(2,1)S(1)}, bf16[512,1024]{1,0:T(8,128)(2,1)S(1)}, u32[]{:S(2)}, u32[]{:S(2)}) %collective-permute-start.18) | collective-permute-done | bytes 1048608 | tf_op jit(solution)/shard_map/ppermute | solution.py:179
  208.4 2.9 %shard_map.91 = bf16[512,2048]{1,0:T(8,128)(2,1)} custom-call(s32[2]{0:T(128)S(1)} %pad_add_fusion.refs_0_, bf16[512,1024]{1,0:T(8,128)(2,1)S(1)} %bitcast.12, bf16[512,1024]{1,0:T(8,128)(2,1)S(1)} %collective-permute-done.18.refs_2_, f32[16,128]{1,0:T(8,128)S(1)} %bitcast.13, f32[16,128]{1,0:T(8,128)S(1)} %bitcast.14), custom_call_target="tpu_custom_call" | custom-call | tf_op jit(solution)/shard_map/pallas_call | solution.py:68
  (54 shorter events, 4.0 us)
Async XLA Ops:
  2.1 47.6 %copy-start.3 = (f32[2048]{0:T(1024)S(1)}, f32[2048]{0:T(1024)}, u32[]{:S(2)}) copy-start(f32[2048]{0:T(1024)} %param.10) | copy-start | bytes 24580
  2.2 54.7 %collective-permute-start.8 = (bf16[1056,128]{1,0:T(8,128)(2,1)S(1)}, bf16[1056,128]{1,0:T(8,128)(2,1)S(1)}, u32[]{:S(2)}, u32[]{:S(2)}) collective-permute-start(bf16[1056,128]{1,0:T(8,128)(2,1)S(1)} %pad_maximum_fusion), channel_id=1, source_target_pairs={{0,241},{1,0},{2,243},{3,2},{4,245},{5,4},{6,247},{7,6},{8,249},{9... | collective-permute-start | bytes 811016 | tf_op jit(solution)/shard_map/ppermute | solution.py:112
  43.6 8.1 %collective-permute-start = (bf16[1056,128]{1,0:T(8,128)(2,1)S(1)}, bf16[1056,128]{1,0:T(8,128)(2,1)S(1)}, u32[]{:S(2)}, u32[]{:S(2)}) collective-permute-start(bf16[1056,128]{1,0:T(8,128)(2,1)S(1)} %pad_maximum_fusion), channel_id=1, source_target_pairs={{1,241},{3,243},{5,245},{7,247},{9,249},{11,251},{13,253},{15,255}... | collective-permute-start | bytes 811016 | tf_op jit(solution)/shard_map/ppermute | solution.py:113
  47.5 11.5 %copy-start.2 = (bf16[512,2048]{1,0:T(8,128)(2,1)S(1)}, bf16[512,2048]{1,0:T(8,128)(2,1)}, u32[]{:S(2)}) copy-start(bf16[512,2048]{1,0:T(8,128)(2,1)} %param.9) | copy-start | bytes 6291460
  51.8 8.4 %collective-permute-start.1 = (bf16[1056,128]{1,0:T(8,128)(2,1)S(1)}, bf16[1056,128]{1,0:T(8,128)(2,1)S(1)}, u32[]{:S(2)}, u32[]{:S(2)}) collective-permute-start(bf16[1056,128]{1,0:T(8,128)(2,1)S(1)} %broadcast_select_fusion), channel_id=1, source_target_pairs={{0,16},{1,241},{2,18},{3,243},{4,20},{5,245},{6,22},{7,247},{8,24}... | collective-permute-start | bytes 811016 | tf_op jit(solution)/shard_map/ppermute | solution.py:139
  57.0 7.2 %collective-permute-start.9 = (bf16[1056,128]{1,0:T(8,128)(2,1)S(1)}, bf16[1056,128]{1,0:T(8,128)(2,1)S(1)}, u32[]{:S(2)}, u32[]{:S(2)}) collective-permute-start(bf16[1056,128]{1,0:T(8,128)(2,1)S(1)} %collective-permute-done.8), channel_id=1, source_target_pairs={{0,16},{1,241},{2,18},{3,243},{4,20},{5,245},{6,22},{7,247},{8,24}... | collective-permute-start | bytes 811016 | tf_op jit(solution)/shard_map/ppermute | solution.py:139
  64.3 7.5 %collective-permute-start.10 = (bf16[1056,128]{1,0:T(8,128)(2,1)S(1)}, bf16[1056,128]{1,0:T(8,128)(2,1)S(1)}, u32[]{:S(2)}, u32[]{:S(2)}) collective-permute-start(bf16[1056,128]{1,0:T(8,128)(2,1)S(1)} %collective-permute-done.9), channel_id=1, source_target_pairs={{0,16},{1,241},{2,18},{3,243},{4,20},{5,245},{6,22},{7,247},{8,24}... | collective-permute-start | bytes 811016 | tf_op jit(solution)/shard_map/ppermute | solution.py:139
  68.3 7.2 %collective-permute-start.2 = (bf16[1056,128]{1,0:T(8,128)(2,1)S(1)}, bf16[1056,128]{1,0:T(8,128)(2,1)S(1)}, u32[]{:S(2)}, u32[]{:S(2)}) collective-permute-start(bf16[1056,128]{1,0:T(8,128)(2,1)S(1)} %collective-permute-done.1), channel_id=1, source_target_pairs={{0,16},{1,241},{2,18},{3,243},{4,20},{5,245},{6,22},{7,247},{8,24}... | collective-permute-start | bytes 811016 | tf_op jit(solution)/shard_map/ppermute | solution.py:139
  75.6 7.5 %collective-permute-start.11 = (bf16[1056,128]{1,0:T(8,128)(2,1)S(1)}, bf16[1056,128]{1,0:T(8,128)(2,1)S(1)}, u32[]{:S(2)}, u32[]{:S(2)}) collective-permute-start(bf16[1056,128]{1,0:T(8,128)(2,1)S(1)} %collective-permute-done.10), channel_id=1, source_target_pairs={{0,16},{1,241},{2,18},{3,243},{4,20},{5,245},{6,22},{7,247},{8,24}... | collective-permute-start | bytes 811016 | tf_op jit(solution)/shard_map/ppermute | solution.py:139
  79.7 7.2 %collective-permute-start.3 = (bf16[1056,128]{1,0:T(8,128)(2,1)S(1)}, bf16[1056,128]{1,0:T(8,128)(2,1)S(1)}, u32[]{:S(2)}, u32[]{:S(2)}) collective-permute-start(bf16[1056,128]{1,0:T(8,128)(2,1)S(1)} %collective-permute-done.2), channel_id=1, source_target_pairs={{0,16},{1,241},{2,18},{3,243},{4,20},{5,245},{6,22},{7,247},{8,24}... | collective-permute-start | bytes 811016 | tf_op jit(solution)/shard_map/ppermute | solution.py:139
  87.0 7.5 %collective-permute-start.12 = (bf16[1056,128]{1,0:T(8,128)(2,1)S(1)}, bf16[1056,128]{1,0:T(8,128)(2,1)S(1)}, u32[]{:S(2)}, u32[]{:S(2)}) collective-permute-start(bf16[1056,128]{1,0:T(8,128)(2,1)S(1)} %collective-permute-done.11), channel_id=1, source_target_pairs={{0,16},{1,241},{2,18},{3,243},{4,20},{5,245},{6,22},{7,247},{8,24}... | collective-permute-start | bytes 811016 | tf_op jit(solution)/shard_map/ppermute | solution.py:139
  91.1 8.5 %collective-permute-start.4 = (bf16[1056,128]{1,0:T(8,128)(2,1)S(1)}, bf16[1056,128]{1,0:T(8,128)(2,1)S(1)}, u32[]{:S(2)}, u32[]{:S(2)}) collective-permute-start(bf16[1056,128]{1,0:T(8,128)(2,1)S(1)} %collective-permute-done.3), channel_id=1, source_target_pairs={{0,16},{1,241},{2,18},{3,243},{4,20},{5,245},{6,22},{7,247},{8,24}... | collective-permute-start | bytes 811016 | tf_op jit(solution)/shard_map/ppermute | solution.py:139
  94.5 8.8 %collective-permute-start.13 = (bf16[1056,128]{1,0:T(8,128)(2,1)S(1)}, bf16[1056,128]{1,0:T(8,128)(2,1)S(1)}, u32[]{:S(2)}, u32[]{:S(2)}) collective-permute-start(bf16[1056,128]{1,0:T(8,128)(2,1)S(1)} %collective-permute-done.12), channel_id=1, source_target_pairs={{0,16},{1,241},{2,18},{3,243},{4,20},{5,245},{6,22},{7,247},{8,24}... | collective-permute-start | bytes 811016 | tf_op jit(solution)/shard_map/ppermute | solution.py:139
  99.6 8.4 %collective-permute-start.5 = (bf16[1056,128]{1,0:T(8,128)(2,1)S(1)}, bf16[1056,128]{1,0:T(8,128)(2,1)S(1)}, u32[]{:S(2)}, u32[]{:S(2)}) collective-permute-start(bf16[1056,128]{1,0:T(8,128)(2,1)S(1)} %collective-permute-done.4), channel_id=1, source_target_pairs={{0,16},{1,241},{2,18},{3,243},{4,20},{5,245},{6,22},{7,247},{8,24}... | collective-permute-start | bytes 811016 | tf_op jit(solution)/shard_map/ppermute | solution.py:139
  103.4 8.4 %collective-permute-start.14 = (bf16[1056,128]{1,0:T(8,128)(2,1)S(1)}, bf16[1056,128]{1,0:T(8,128)(2,1)S(1)}, u32[]{:S(2)}, u32[]{:S(2)}) collective-permute-start(bf16[1056,128]{1,0:T(8,128)(2,1)S(1)} %collective-permute-done.13), channel_id=1, source_target_pairs={{0,16},{1,241},{2,18},{3,243},{4,20},{5,245},{6,22},{7,247},{8,24}... | collective-permute-start | bytes 811016 | tf_op jit(solution)/shard_map/ppermute | solution.py:139
  108.0 8.4 %collective-permute-start.6 = (bf16[1056,128]{1,0:T(8,128)(2,1)S(1)}, bf16[1056,128]{1,0:T(8,128)(2,1)S(1)}, u32[]{:S(2)}, u32[]{:S(2)}) collective-permute-start(bf16[1056,128]{1,0:T(8,128)(2,1)S(1)} %collective-permute-done.5), channel_id=1, source_target_pairs={{0,16},{1,241},{2,18},{3,243},{4,20},{5,245},{6,22},{7,247},{8,24}... | collective-permute-start | bytes 811016 | tf_op jit(solution)/shard_map/ppermute | solution.py:139
  111.8 18.0 %collective-permute-start.15 = (bf16[1056,128]{1,0:T(8,128)(2,1)S(1)}, bf16[1056,128]{1,0:T(8,128)(2,1)S(1)}, u32[]{:S(2)}, u32[]{:S(2)}) collective-permute-start(bf16[1056,128]{1,0:T(8,128)(2,1)S(1)} %collective-permute-done.14), channel_id=1, source_target_pairs={{0,16},{1,241},{2,18},{3,243},{4,20},{5,245},{6,22},{7,247},{8,24}... | collective-permute-start | bytes 811016 | tf_op jit(solution)/shard_map/ppermute | solution.py:139
  116.4 7.5 %collective-permute-start.7 = (bf16[1056,128]{1,0:T(8,128)(2,1)S(1)}, bf16[1056,128]{1,0:T(8,128)(2,1)S(1)}, u32[]{:S(2)}, u32[]{:S(2)}) collective-permute-start(bf16[1056,128]{1,0:T(8,128)(2,1)S(1)} %collective-permute-done.6), channel_id=1, source_target_pairs={{0,16},{1,241},{2,18},{3,243},{4,20},{5,245},{6,22},{7,247},{8,24}... | collective-permute-start | bytes 811016 | tf_op jit(solution)/shard_map/ppermute | solution.py:139
  124.4 8.2 %collective-permute-start.17 = (bf16[704,512]{1,0:T(8,128)(2,1)S(1)}, bf16[704,512]{1,0:T(8,128)(2,1)S(1)}, u32[]{:S(2)}, u32[]{:S(2)}) collective-permute-start(bf16[704,512]{1,0:T(8,128)(2,1)S(1)} %get-tuple-element.13), channel_id=1, source_target_pairs={{0,1},{1,0},{2,3},{3,2},{4,5},{5,4},{6,7},{7,6},{8,9},{9,8},{10,11... | collective-permute-start | bytes 2162696 | tf_op jit(solution)/shard_map/ppermute | solution.py:145
  130.3 4.1 %collective-permute-start.16 = (bf16[704,512]{1,0:T(8,128)(2,1)S(1)}, bf16[704,512]{1,0:T(8,128)(2,1)S(1)}, u32[]{:S(2)}, u32[]{:S(2)}) collective-permute-start(bf16[704,512]{1,0:T(8,128)(2,1)S(1)} %get-tuple-element.15), channel_id=1, source_target_pairs={{0,1},{1,0},{2,3},{3,2},{4,5},{5,4},{6,7},{7,6},{8,9},{9,8},{10,11... | collective-permute-start | bytes 2162696 | tf_op jit(solution)/shard_map/ppermute | solution.py:146
  171.9 36.5 %copy-start = (f32[2048]{0:T(1024)S(1)}, f32[2048]{0:T(1024)}, u32[]{:S(2)}) copy-start(f32[2048]{0:T(1024)} %param.16) | copy-start | bytes 24580
  171.9 36.5 %copy-start.1 = (f32[2048]{0:T(1024)S(1)}, f32[2048]{0:T(1024)}, u32[]{:S(2)}) copy-start(f32[2048]{0:T(1024)} %param.17) | copy-start | bytes 24580
  203.0 5.3 %collective-permute-start.18 = (bf16[512,1024]{1,0:T(8,128)(2,1)S(1)}, bf16[512,1024]{1,0:T(8,128)(2,1)S(1)}, u32[]{:S(2)}, u32[]{:S(2)}) collective-permute-start(bf16[512,1024]{1,0:T(8,128)(2,1)S(1)} %bitcast.11), channel_id=1, source_target_pairs={{0,1},{1,0},{2,3},{3,2},{4,5},{5,4},{6,7},{7,6},{8,9},{9,8},{10,11... | collective-permute-start | bytes 3145736 | tf_op jit(solution)/shard_map/ppermute | solution.py:179

commit v3 on v0

--- a/solution.py
+++ b/solution.py
@@ -146,8 +146,9 @@
     arrived = lax.ppermute(sums, "tp", partner)
 
     def gated(sums, more):
-        sums = sums + more.astype(jnp.float32)
-        return (jax.nn.silu(sums[:units]) * sums[units:]).astype(low)
+        gate = sums[:units] + more[:units].astype(jnp.float32)
+        up = sums[units:] + more[units:].astype(jnp.float32)
+        return (jax.nn.silu(gate) * up).astype(low)
 
     hidden = jnp.concatenate(
         [gated(sum_own, arrived[2 * units :]), gated(sum_other, arrived[: 2 * units])], axis=0

time: 204 us -> 204 us (level)
  no operation moved by 1% of the time
where the time goes in v3:
time: 204 us; the launch traced here: 203 us
  starting transfers between devices  104 us (51%)
  blocking collectives  63.6 us (31%)
  waiting for transfers between devices  17.3 us (8%)
  matrix products  8.3 us (4%)
  other arithmetic  5.63 us (3%)
  Pallas kernels  2.95 us (1%)
    all_to_all x2, blocking collectives, over_chips(): lax.all_to_all(array, 'tp', 0, 0, axis_index_groups=chips, tiled=True)  63.6 us
    ppermute x14, starting transfers between devices, body(): held[chain] = lax.ppermute(held[chain], both, ring)  48.4 us
    ppermute x1, starting transfers between devices, body(): other0 = lax.ppermute(packed, both, enter)  41.5 us
    ppermute x14, waiting for transfers between devices, body(): held[chain] = lax.ppermute(held[chain], both, ring)  10.8 us
    dot_general x16, matrix products, product(): lax.dot_general(weights, k_normed, (((1,), (1,)), ((), ())), preferred_el...  7.3 us
    ppermute x1, starting transfers between devices, body(): other = lax.ppermute(mine, 'tp', partner)  5.25 us
    ppermute x1, starting transfers between devices, body(): arrived = lax.ppermute(sums, 'tp', partner)  5.11 us
  transfers between devices with their start and end apart: 18, of which 7 were waited for; matrix products, arithmetic and copies ran while one was open for 5% of the time, Pallas kernels for 0%

profile of v3, /device:TPU:65, one launch (start us, length us, event | category | flops | bytes accessed | tf_op | source)
XLA Modules:
  0.0 202.9 jit_solution(17889038378146498156)
XLA Ops:
  0.0 0.9 convert_element_type.86
  0.9 1.2 fusion.25
  2.2 41.5 %collective-permute-start.8 = (bf16[1056,128]{1,0:T(8,128)(2,1)S(1)}, bf16[1056,128]{1,0:T(8,128)(2,1)S(1)}, u32[]{:S(2)}, u32[]{:S(2)}) collective-permute-start(bf16[1056,128]{1,0:T(8,128)(2,1)S(1)} %pad_maximum_fusion.1), channel_id=1, source_target_pairs={{0,241},{1,0},{2,243},{3,2},{4,245},{5,4},{6,247},{7,6},{8,249},{9... | collective-permute-start | bytes 811016 | tf_op jit(solution)/shard_map/ppermute | solution.py:112
  43.7 3.7 %collective-permute-start = (bf16[1056,128]{1,0:T(8,128)(2,1)S(1)}, bf16[1056,128]{1,0:T(8,128)(2,1)S(1)}, u32[]{:S(2)}, u32[]{:S(2)}) collective-permute-start(bf16[1056,128]{1,0:T(8,128)(2,1)S(1)} %pad_maximum_fusion.1), channel_id=1, source_target_pairs={{1,241},{3,243},{5,245},{7,247},{9,249},{11,251},{13,253},{15,255}... | collective-permute-start | bytes 811016 | tf_op jit(solution)/shard_map/ppermute | solution.py:113
  47.4 2.1 %multiply_reduce_fusion = f32[512]{0:T(512)S(1)} fusion(bf16[512,2048]{1,0:T(8,128)(2,1)} %param.9), kind=kLoop, calls=%fused_computation | loop fusion | flops 3145216 | bytes 2099200 | tf_op jit(solution)/shard_map/reduce_sum | solution.py:117
  49.6 2.2 %collective-permute-done = bf16[1056,128]{1,0:T(8,128)(2,1)S(1)} collective-permute-done((bf16[1056,128]{1,0:T(8,128)(2,1)S(1)}, bf16[1056,128]{1,0:T(8,128)(2,1)S(1)}, u32[]{:S(2)}, u32[]{:S(2)}) %collective-permute-start) | collective-permute-done | bytes 270368 | tf_op jit(solution)/shard_map/ppermute | solution.py:113
  51.8 5.1 %collective-permute-start.1 = (bf16[1056,128]{1,0:T(8,128)(2,1)S(1)}, bf16[1056,128]{1,0:T(8,128)(2,1)S(1)}, u32[]{:S(2)}, u32[]{:S(2)}) collective-permute-start(bf16[1056,128]{1,0:T(8,128)(2,1)S(1)} %broadcast_select_fusion), channel_id=1, source_target_pairs={{0,16},{1,241},{2,18},{3,243},{4,20},{5,245},{6,22},{7,247},{8,24}... | collective-permute-start | bytes 811016 | tf_op jit(solution)/shard_map/ppermute | solution.py:139
  57.0 1.9 collective-permute-start.9
  59.4 0.8 collective-permute-done.1
  60.3 5.0 %collective-permute-start.2 = (bf16[1056,128]{1,0:T(8,128)(2,1)S(1)}, bf16[1056,128]{1,0:T(8,128)(2,1)S(1)}, u32[]{:S(2)}, u32[]{:S(2)}) collective-permute-start(bf16[1056,128]{1,0:T(8,128)(2,1)S(1)} %collective-permute-done.1), channel_id=1, source_target_pairs={{0,16},{1,241},{2,18},{3,243},{4,20},{5,245},{6,22},{7,247},{8,24}... | collective-permute-start | bytes 811016 | tf_op jit(solution)/shard_map/ppermute | solution.py:139
  65.3 0.5 fusion.22
  65.8 0.5 convolution_add_fusion.13
  66.2 2.0 collective-permute-start.10
  68.2 0.5 convolution_add_fusion.6
  68.7 4.8 %collective-permute-done.10 = bf16[1056,128]{1,0:T(8,128)(2,1)S(1)} collective-permute-done((bf16[1056,128]{1,0:T(8,128)(2,1)S(1)}, bf16[1056,128]{1,0:T(8,128)(2,1)S(1)}, u32[]{:S(2)}, u32[]{:S(2)}) %collective-permute-start.10) | collective-permute-done | bytes 270368 | tf_op jit(solution)/shard_map/ppermute | solution.py:139
  73.5 3.1 %collective-permute-start.11 = (bf16[1056,128]{1,0:T(8,128)(2,1)S(1)}, bf16[1056,128]{1,0:T(8,128)(2,1)S(1)}, u32[]{:S(2)}, u32[]{:S(2)}) collective-permute-start(bf16[1056,128]{1,0:T(8,128)(2,1)S(1)} %collective-permute-done.10), channel_id=1, source_target_pairs={{0,16},{1,241},{2,18},{3,243},{4,20},{5,245},{6,22},{7,247},{8,24}... | collective-permute-start | bytes 811016 | tf_op jit(solution)/shard_map/ppermute | solution.py:139
  76.6 2.0 collective-permute-start.3
  78.6 0.5 convolution_add_fusion.12
  79.1 0.5 convolution_add_fusion.5
  79.5 1.5 collective-permute-done.11
  81.0 4.1 %collective-permute-start.12 = (bf16[1056,128]{1,0:T(8,128)(2,1)S(1)}, bf16[1056,128]{1,0:T(8,128)(2,1)S(1)}, u32[]{:S(2)}, u32[]{:S(2)}) collective-permute-start(bf16[1056,128]{1,0:T(8,128)(2,1)S(1)} %collective-permute-done.11), channel_id=1, source_target_pairs={{0,16},{1,241},{2,18},{3,243},{4,20},{5,245},{6,22},{7,247},{8,24}... | collective-permute-start | bytes 811016 | tf_op jit(solution)/shard_map/ppermute | solution.py:139
  85.1 2.9 %collective-permute-start.4 = (bf16[1056,128]{1,0:T(8,128)(2,1)S(1)}, bf16[1056,128]{1,0:T(8,128)(2,1)S(1)}, u32[]{:S(2)}, u32[]{:S(2)}) collective-permute-start(bf16[1056,128]{1,0:T(8,128)(2,1)S(1)} %collective-permute-done.3), channel_id=1, source_target_pairs={{0,16},{1,241},{2,18},{3,243},{4,20},{5,245},{6,22},{7,247},{8,24}... | collective-permute-start | bytes 811016 | tf_op jit(solution)/shard_map/ppermute | solution.py:139
  88.0 0.5 convolution_add_fusion.11
  88.4 0.5 convolution_add_fusion.4
  88.9 4.6 %collective-permute-start.13 = (bf16[1056,128]{1,0:T(8,128)(2,1)S(1)}, bf16[1056,128]{1,0:T(8,128)(2,1)S(1)}, u32[]{:S(2)}, u32[]{:S(2)}) collective-permute-start(bf16[1056,128]{1,0:T(8,128)(2,1)S(1)} %collective-permute-done.12), channel_id=1, source_target_pairs={{0,16},{1,241},{2,18},{3,243},{4,20},{5,245},{6,22},{7,247},{8,24}... | collective-permute-start | bytes 811016 | tf_op jit(solution)/shard_map/ppermute | solution.py:139
  93.5 2.9 %collective-permute-start.5 = (bf16[1056,128]{1,0:T(8,128)(2,1)S(1)}, bf16[1056,128]{1,0:T(8,128)(2,1)S(1)}, u32[]{:S(2)}, u32[]{:S(2)}) collective-permute-start(bf16[1056,128]{1,0:T(8,128)(2,1)S(1)} %collective-permute-done.4), channel_id=1, source_target_pairs={{0,16},{1,241},{2,18},{3,243},{4,20},{5,245},{6,22},{7,247},{8,24}... | collective-permute-start | bytes 811016 | tf_op jit(solution)/shard_map/ppermute | solution.py:139
  96.4 0.5 convolution_add_fusion.10
  96.9 0.5 convolution_add_fusion.3
  97.3 4.6 %collective-permute-start.14 = (bf16[1056,128]{1,0:T(8,128)(2,1)S(1)}, bf16[1056,128]{1,0:T(8,128)(2,1)S(1)}, u32[]{:S(2)}, u32[]{:S(2)}) collective-permute-start(bf16[1056,128]{1,0:T(8,128)(2,1)S(1)} %collective-permute-done.13), channel_id=1, source_target_pairs={{0,16},{1,241},{2,18},{3,243},{4,20},{5,245},{6,22},{7,247},{8,24}... | collective-permute-start | bytes 811016 | tf_op jit(solution)/shard_map/ppermute | solution.py:139
  101.9 2.9 %collective-permute-start.6 = (bf16[1056,128]{1,0:T(8,128)(2,1)S(1)}, bf16[1056,128]{1,0:T(8,128)(2,1)S(1)}, u32[]{:S(2)}, u32[]{:S(2)}) collective-permute-start(bf16[1056,128]{1,0:T(8,128)(2,1)S(1)} %collective-permute-done.5), channel_id=1, source_target_pairs={{0,16},{1,241},{2,18},{3,243},{4,20},{5,245},{6,22},{7,247},{8,24}... | collective-permute-start | bytes 811016 | tf_op jit(solution)/shard_map/ppermute | solution.py:139
  104.8 0.5 convolution_add_fusion.9
  105.3 0.5 convolution_add_fusion.2
  105.8 4.6 %collective-permute-start.15 = (bf16[1056,128]{1,0:T(8,128)(2,1)S(1)}, bf16[1056,128]{1,0:T(8,128)(2,1)S(1)}, u32[]{:S(2)}, u32[]{:S(2)}) collective-permute-start(bf16[1056,128]{1,0:T(8,128)(2,1)S(1)} %collective-permute-done.14), channel_id=1, source_target_pairs={{0,16},{1,241},{2,18},{3,243},{4,20},{5,245},{6,22},{7,247},{8,24}... | collective-permute-start | bytes 811016 | tf_op jit(solution)/shard_map/ppermute | solution.py:139
  110.4 2.9 %collective-permute-start.7 = (bf16[1056,128]{1,0:T(8,128)(2,1)S(1)}, bf16[1056,128]{1,0:T(8,128)(2,1)S(1)}, u32[]{:S(2)}, u32[]{:S(2)}) collective-permute-start(bf16[1056,128]{1,0:T(8,128)(2,1)S(1)} %collective-permute-done.6), channel_id=1, source_target_pairs={{0,16},{1,241},{2,18},{3,243},{4,20},{5,245},{6,22},{7,247},{8,24}... | collective-permute-start | bytes 811016 | tf_op jit(solution)/shard_map/ppermute | solution.py:139
  113.3 0.5 convolution_add_fusion.8
  113.7 0.5 convolution_add_fusion.1
  114.2 3.7 %collective-permute-done.7 = bf16[1056,128]{1,0:T(8,128)(2,1)S(1)} collective-permute-done((bf16[1056,128]{1,0:T(8,128)(2,1)S(1)}, bf16[1056,128]{1,0:T(8,128)(2,1)S(1)}, u32[]{:S(2)}, u32[]{:S(2)}) %collective-permute-start.7) | collective-permute-done | bytes 270368 | tf_op jit(solution)/shard_map/ppermute | solution.py:139
  117.9 0.5 fusion.46
  118.4 0.5 fusion.45
  119.0 5.1 %collective-permute-start.16 = (bf16[1408,512]{1,0:T(8,128)(2,1)S(1)}, bf16[1408,512]{1,0:T(8,128)(2,1)S(1)}, u32[]{:S(2)}, u32[]{:S(2)}) collective-permute-start(bf16[1408,512]{1,0:T(8,128)(2,1)S(1)} %pad_maximum_fusion), channel_id=1, source_target_pairs={{0,1},{1,0},{2,3},{3,2},{4,5},{5,4},{6,7},{7,6},{8,9},{9,8},{10,11... | collective-permute-start | bytes 4325384 | tf_op jit(solution)/shard_map/ppermute | solution.py:146
  124.8 2.1 %collective-permute-done.16 = bf16[1408,512]{1,0:T(8,128)(2,1)S(1)} collective-permute-done((bf16[1408,512]{1,0:T(8,128)(2,1)S(1)}, bf16[1408,512]{1,0:T(8,128)(2,1)S(1)}, u32[]{:S(2)}, u32[]{:S(2)}) %collective-permute-start.16) | collective-permute-done | bytes 1441824 | tf_op jit(solution)/shard_map/ppermute | solution.py:146
  126.9 0.6 fusion.3
  127.5 1.0 convolution_convert_fusion
  128.5 34.8 %all_to_all.10 = bf16[8,64,1024]{2,1,0:T(8,128)(2,1)S(1)} all-to-all(bf16[8,64,1024]{2,1,0:T(8,128)(2,1)S(1)} %bitcast.15), channel_id=1, replica_groups={{0,2,4,6,8,10,12,14},{1,3,5,7,9,11,13,15},{16,18,20,22,24,26,28,30},{17..., dimensions={0} | all-to-all | bytes 2097152 | tf_op jit(solution)/shard_map/all_to_all | solution.py:164
  163.6 28.8 %all_to_all.11 = bf16[8,64,1024]{2,1,0:T(8,128)(2,1)S(1)} all-to-all(bf16[8,64,1024]{2,1,0:T(8,128)(2,1)S(1)} %broadcast_in_dim.2), channel_id=1, replica_groups={{0,2,4,6,8,10,12,14},{1,3,5,7,9,11,13,15},{16,18,20,22,24,26,28,30},{17..., dimensions={0} | all-to-all | bytes 2097152 | tf_op jit(solution)/shard_map/all_to_all | solution.py:164
  192.4 5.2 %collective-permute-start.17 = (bf16[512,1024]{1,0:T(8,128)(2,1)S(1)}, bf16[512,1024]{1,0:T(8,128)(2,1)S(1)}, u32[]{:S(2)}, u32[]{:S(2)}) collective-permute-start(bf16[512,1024]{1,0:T(8,128)(2,1)S(1)} %bitcast.11), channel_id=1, source_target_pairs={{0,1},{1,0},{2,3},{3,2},{4,5},{5,4},{6,7},{7,6},{8,9},{9,8},{10,11... | collective-permute-start | bytes 3145736 | tf_op jit(solution)/shard_map/ppermute | solution.py:181
  197.8 2.2 %collective-permute-done.17.refs_2_ = bf16[512,1024]{1,0:T(8,128)(2,1)S(1)} collective-permute-done((bf16[512,1024]{1,0:T(8,128)(2,1)S(1)}, bf16[512,1024]{1,0:T(8,128)(2,1)S(1)}, u32[]{:S(2)}, u32[]{:S(2)}) %collective-permute-start.17) | collective-permute-done | bytes 1048608 | tf_op jit(solution)/shard_map/ppermute | solution.py:181
  199.9 2.9 %shard_map.91 = bf16[512,2048]{1,0:T(8,128)(2,1)} custom-call(s32[2]{0:T(128)S(1)} %pad_add_fusion.refs_0_, bf16[512,1024]{1,0:T(8,128)(2,1)S(1)} %bitcast.12, bf16[512,1024]{1,0:T(8,128)(2,1)S(1)} %collective-permute-done.17.refs_2_, f32[16,128]{1,0:T(8,128)S(1)} %bitcast.13, f32[16,128]{1,0:T(8,128)S(1)} %bitcast.14), custom_call_target="tpu_custom_call" | custom-call | tf_op jit(solution)/shard_map/pallas_call | solution.py:68
  (52 shorter events, 1.7 us)
Async XLA Ops:
  2.2 54.7 %copy-start.3 = (f32[2048]{0:T(1024)S(1)}, f32[2048]{0:T(1024)}, u32[]{:S(2)}) copy-start(f32[2048]{0:T(1024)} %param.10) | copy-start | bytes 24580
  2.2 56.8 %copy-start.2 = (bf16[512,2048]{1,0:T(8,128)(2,1)S(1)}, bf16[512,2048]{1,0:T(8,128)(2,1)}, u32[]{:S(2)}) copy-start(bf16[512,2048]{1,0:T(8,128)(2,1)} %param.9) | copy-start | bytes 6291460
  2.2 54.8 %collective-permute-start.8 = (bf16[1056,128]{1,0:T(8,128)(2,1)S(1)}, bf16[1056,128]{1,0:T(8,128)(2,1)S(1)}, u32[]{:S(2)}, u32[]{:S(2)}) collective-permute-start(bf16[1056,128]{1,0:T(8,128)(2,1)S(1)} %pad_maximum_fusion.1), channel_id=1, source_target_pairs={{0,241},{1,0},{2,243},{3,2},{4,245},{5,4},{6,247},{7,6},{8,249},{9... | collective-permute-start | bytes 811016 | tf_op jit(solution)/shard_map/ppermute | solution.py:112
  43.7 8.1 %collective-permute-start = (bf16[1056,128]{1,0:T(8,128)(2,1)S(1)}, bf16[1056,128]{1,0:T(8,128)(2,1)S(1)}, u32[]{:S(2)}, u32[]{:S(2)}) collective-permute-start(bf16[1056,128]{1,0:T(8,128)(2,1)S(1)} %pad_maximum_fusion.1), channel_id=1, source_target_pairs={{1,241},{3,243},{5,245},{7,247},{9,249},{11,251},{13,253},{15,255}... | collective-permute-start | bytes 811016 | tf_op jit(solution)/shard_map/ppermute | solution.py:113
  51.8 8.4 %collective-permute-start.1 = (bf16[1056,128]{1,0:T(8,128)(2,1)S(1)}, bf16[1056,128]{1,0:T(8,128)(2,1)S(1)}, u32[]{:S(2)}, u32[]{:S(2)}) collective-permute-start(bf16[1056,128]{1,0:T(8,128)(2,1)S(1)} %broadcast_select_fusion), channel_id=1, source_target_pairs={{0,16},{1,241},{2,18},{3,243},{4,20},{5,245},{6,22},{7,247},{8,24}... | collective-permute-start | bytes 811016 | tf_op jit(solution)/shard_map/ppermute | solution.py:139
  57.0 9.2 %collective-permute-start.9 = (bf16[1056,128]{1,0:T(8,128)(2,1)S(1)}, bf16[1056,128]{1,0:T(8,128)(2,1)S(1)}, u32[]{:S(2)}, u32[]{:S(2)}) collective-permute-start(bf16[1056,128]{1,0:T(8,128)(2,1)S(1)} %collective-permute-done.8), channel_id=1, source_target_pairs={{0,16},{1,241},{2,18},{3,243},{4,20},{5,245},{6,22},{7,247},{8,24}... | collective-permute-start | bytes 811016 | tf_op jit(solution)/shard_map/ppermute | solution.py:139
  60.3 16.4 %collective-permute-start.2 = (bf16[1056,128]{1,0:T(8,128)(2,1)S(1)}, bf16[1056,128]{1,0:T(8,128)(2,1)S(1)}, u32[]{:S(2)}, u32[]{:S(2)}) collective-permute-start(bf16[1056,128]{1,0:T(8,128)(2,1)S(1)} %collective-permute-done.1), channel_id=1, source_target_pairs={{0,16},{1,241},{2,18},{3,243},{4,20},{5,245},{6,22},{7,247},{8,24}... | collective-permute-start | bytes 811016 | tf_op jit(solution)/shard_map/ppermute | solution.py:139
  66.2 7.2 %collective-permute-start.10 = (bf16[1056,128]{1,0:T(8,128)(2,1)S(1)}, bf16[1056,128]{1,0:T(8,128)(2,1)S(1)}, u32[]{:S(2)}, u32[]{:S(2)}) collective-permute-start(bf16[1056,128]{1,0:T(8,128)(2,1)S(1)} %collective-permute-done.9), channel_id=1, source_target_pairs={{0,16},{1,241},{2,18},{3,243},{4,20},{5,245},{6,22},{7,247},{8,24}... | collective-permute-start | bytes 811016 | tf_op jit(solution)/shard_map/ppermute | solution.py:139
  73.5 7.5 %collective-permute-start.11 = (bf16[1056,128]{1,0:T(8,128)(2,1)S(1)}, bf16[1056,128]{1,0:T(8,128)(2,1)S(1)}, u32[]{:S(2)}, u32[]{:S(2)}) collective-permute-start(bf16[1056,128]{1,0:T(8,128)(2,1)S(1)} %collective-permute-done.10), channel_id=1, source_target_pairs={{0,16},{1,241},{2,18},{3,243},{4,20},{5,245},{6,22},{7,247},{8,24}... | collective-permute-start | bytes 811016 | tf_op jit(solution)/shard_map/ppermute | solution.py:139
  76.6 8.4 %collective-permute-start.3 = (bf16[1056,128]{1,0:T(8,128)(2,1)S(1)}, bf16[1056,128]{1,0:T(8,128)(2,1)S(1)}, u32[]{:S(2)}, u32[]{:S(2)}) collective-permute-start(bf16[1056,128]{1,0:T(8,128)(2,1)S(1)} %collective-permute-done.2), channel_id=1, source_target_pairs={{0,16},{1,241},{2,18},{3,243},{4,20},{5,245},{6,22},{7,247},{8,24}... | collective-permute-start | bytes 811016 | tf_op jit(solution)/shard_map/ppermute | solution.py:139
  81.0 7.9 %collective-permute-start.12 = (bf16[1056,128]{1,0:T(8,128)(2,1)S(1)}, bf16[1056,128]{1,0:T(8,128)(2,1)S(1)}, u32[]{:S(2)}, u32[]{:S(2)}) collective-permute-start(bf16[1056,128]{1,0:T(8,128)(2,1)S(1)} %collective-permute-done.11), channel_id=1, source_target_pairs={{0,16},{1,241},{2,18},{3,243},{4,20},{5,245},{6,22},{7,247},{8,24}... | collective-permute-start | bytes 811016 | tf_op jit(solution)/shard_map/ppermute | solution.py:139
  85.1 8.4 %collective-permute-start.4 = (bf16[1056,128]{1,0:T(8,128)(2,1)S(1)}, bf16[1056,128]{1,0:T(8,128)(2,1)S(1)}, u32[]{:S(2)}, u32[]{:S(2)}) collective-permute-start(bf16[1056,128]{1,0:T(8,128)(2,1)S(1)} %collective-permute-done.3), channel_id=1, source_target_pairs={{0,16},{1,241},{2,18},{3,243},{4,20},{5,245},{6,22},{7,247},{8,24}... | collective-permute-start | bytes 811016 | tf_op jit(solution)/shard_map/ppermute | solution.py:139
  88.9 8.4 %collective-permute-start.13 = (bf16[1056,128]{1,0:T(8,128)(2,1)S(1)}, bf16[1056,128]{1,0:T(8,128)(2,1)S(1)}, u32[]{:S(2)}, u32[]{:S(2)}) collective-permute-start(bf16[1056,128]{1,0:T(8,128)(2,1)S(1)} %collective-permute-done.12), channel_id=1, source_target_pairs={{0,16},{1,241},{2,18},{3,243},{4,20},{5,245},{6,22},{7,247},{8,24}... | collective-permute-start | bytes 811016 | tf_op jit(solution)/shard_map/ppermute | solution.py:139
  93.5 8.4 %collective-permute-start.5 = (bf16[1056,128]{1,0:T(8,128)(2,1)S(1)}, bf16[1056,128]{1,0:T(8,128)(2,1)S(1)}, u32[]{:S(2)}, u32[]{:S(2)}) collective-permute-start(bf16[1056,128]{1,0:T(8,128)(2,1)S(1)} %collective-permute-done.4), channel_id=1, source_target_pairs={{0,16},{1,241},{2,18},{3,243},{4,20},{5,245},{6,22},{7,247},{8,24}... | collective-permute-start | bytes 811016 | tf_op jit(solution)/shard_map/ppermute | solution.py:139
  97.3 8.4 %collective-permute-start.14 = (bf16[1056,128]{1,0:T(8,128)(2,1)S(1)}, bf16[1056,128]{1,0:T(8,128)(2,1)S(1)}, u32[]{:S(2)}, u32[]{:S(2)}) collective-permute-start(bf16[1056,128]{1,0:T(8,128)(2,1)S(1)} %collective-permute-done.13), channel_id=1, source_target_pairs={{0,16},{1,241},{2,18},{3,243},{4,20},{5,245},{6,22},{7,247},{8,24}... | collective-permute-start | bytes 811016 | tf_op jit(solution)/shard_map/ppermute | solution.py:139
  101.9 8.4 %collective-permute-start.6 = (bf16[1056,128]{1,0:T(8,128)(2,1)S(1)}, bf16[1056,128]{1,0:T(8,128)(2,1)S(1)}, u32[]{:S(2)}, u32[]{:S(2)}) collective-permute-start(bf16[1056,128]{1,0:T(8,128)(2,1)S(1)} %collective-permute-done.5), channel_id=1, source_target_pairs={{0,16},{1,241},{2,18},{3,243},{4,20},{5,245},{6,22},{7,247},{8,24}... | collective-permute-start | bytes 811016 | tf_op jit(solution)/shard_map/ppermute | solution.py:139
  105.8 12.6 %collective-permute-start.15 = (bf16[1056,128]{1,0:T(8,128)(2,1)S(1)}, bf16[1056,128]{1,0:T(8,128)(2,1)S(1)}, u32[]{:S(2)}, u32[]{:S(2)}) collective-permute-start(bf16[1056,128]{1,0:T(8,128)(2,1)S(1)} %collective-permute-done.14), channel_id=1, source_target_pairs={{0,16},{1,241},{2,18},{3,243},{4,20},{5,245},{6,22},{7,247},{8,24}... | collective-permute-start | bytes 811016 | tf_op jit(solution)/shard_map/ppermute | solution.py:139
  110.4 7.5 %collective-permute-start.7 = (bf16[1056,128]{1,0:T(8,128)(2,1)S(1)}, bf16[1056,128]{1,0:T(8,128)(2,1)S(1)}, u32[]{:S(2)}, u32[]{:S(2)}) collective-permute-start(bf16[1056,128]{1,0:T(8,128)(2,1)S(1)} %collective-permute-done.6), channel_id=1, source_target_pairs={{0,16},{1,241},{2,18},{3,243},{4,20},{5,245},{6,22},{7,247},{8,24}... | collective-permute-start | bytes 811016 | tf_op jit(solution)/shard_map/ppermute | solution.py:139
  119.0 7.9 %collective-permute-start.16 = (bf16[1408,512]{1,0:T(8,128)(2,1)S(1)}, bf16[1408,512]{1,0:T(8,128)(2,1)S(1)}, u32[]{:S(2)}, u32[]{:S(2)}) collective-permute-start(bf16[1408,512]{1,0:T(8,128)(2,1)S(1)} %pad_maximum_fusion), channel_id=1, source_target_pairs={{0,1},{1,0},{2,3},{3,2},{4,5},{5,4},{6,7},{7,6},{8,9},{9,8},{10,11... | collective-permute-start | bytes 4325384 | tf_op jit(solution)/shard_map/ppermute | solution.py:146
  163.4 36.5 %copy-start = (f32[2048]{0:T(1024)S(1)}, f32[2048]{0:T(1024)}, u32[]{:S(2)}) copy-start(f32[2048]{0:T(1024)} %param.16) | copy-start | bytes 24580
  163.5 36.5 %copy-start.1 = (f32[2048]{0:T(1024)S(1)}, f32[2048]{0:T(1024)}, u32[]{:S(2)}) copy-start(f32[2048]{0:T(1024)} %param.17) | copy-start | bytes 24580
  192.4 7.5 %collective-permute-start.17 = (bf16[512,1024]{1,0:T(8,128)(2,1)S(1)}, bf16[512,1024]{1,0:T(8,128)(2,1)S(1)}, u32[]{:S(2)}, u32[]{:S(2)}) collective-permute-start(bf16[512,1024]{1,0:T(8,128)(2,1)S(1)} %bitcast.11), channel_id=1, source_target_pairs={{0,1},{1,0},{2,3},{3,2},{4,5},{5,4},{6,7},{7,6},{8,9},{9,8},{10,11... | collective-permute-start | bytes 3145736 | tf_op jit(solution)/shard_map/ppermute | solution.py:181
